TPU v7x, 256 devices: a whole 4x4x8 slice. The times are simulated.
256 devices in a mesh: sp: 32 (over z, y), tp: 8 (over x, core).
Axes of the slice: x: 4, y: 4, z: 8, core: 2. Of those that a mesh axis runs over, the one named last changes fastest.
Arguments:
- queries: bfloat16 [16384, 1024], P('sp', 'tp'), may hold values from -6 to 6
- keys: bfloat16 [16384, 1024], P('sp', 'tp'), may hold values from -6 to 6
- values: bfloat16 [16384, 1024], P('sp', 'tp'), may hold values from -12 to 12
- breaks: bfloat16 [16384, 8], P('sp', 'tp'), may hold values from -12 to 0.5
- residual_in: bfloat16 [16384, 2048], P('sp', 'tp'), may hold values from -6 to 6
- out_weight: bfloat16 [1024, 2048], P('tp'), may hold values from -0.1875 to 0.1875
- first_gain: float32 [2048], replicated, may hold values from 0.1 to 1.9
- first_shift: float32 [2048], replicated, may hold values from -2 to 2
- up_weight: bfloat16 [2048, 8192], P('sp', 'tp'), may hold values from -0.125 to 0.125
- down_weight: bfloat16 [2048, 8192], P('sp', 'tp'), may hold values from -0.0625 to 0.0625
- second_gain: float32 [2048], replicated, may hold values from 0.1 to 1.9
- second_shift: float32 [2048], replicated, may hold values from -2 to 2
Outputs:
- layer_out: bfloat16 [16384, 2048], P('sp', 'tp')
All inputs are finite; a program needn't handle non-finite values.
Results may differ from a plain program's by a relative error of at most 0.018.
Values may be sent and summed in bfloat16 or wider, within the bound.
A program may use at most 128 MiB of HBM per device.

v0:
```python
import jax
import jax.numpy as jnp
from jax import lax
from jax.sharding import PartitionSpec as P

D = 2048
KEY_BLOCK = 512


ALPHA = 2.0**0.25
EPSILON = 1e-05


def in_one_piece(arrays, axis, dim, along):
    ends, at = ([], 0)
    for a in arrays[:-1]:
        at += a.shape[along]
        ends.append(at)
    both = jnp.concatenate(arrays, axis=along)
    return tuple(jnp.split(lax.all_gather(both, axis, axis=dim, tiled=True), ends, axis=along))


def from_partner(array, axis, distance):
    return lax.ppermute(array, axis, [(i, i ^ 1 << distance) for i in range(lax.axis_size(axis))])


def copy_for_each(array, axis):
    peers = lax.axis_size(axis)
    return lax.all_to_all(
        jnp.broadcast_to(array[None], (peers, *array.shape)), axis, 0, 0, tiled=True
    )


def over_copies(array, axis):
    everything = copy_for_each(array, axis)
    return jnp.sum(everything, axis=0)


def together(arrays, axis):
    ends = [0]
    for a in arrays:
        ends.append(ends[-1] + a.size)
    running = over_copies(jnp.concatenate([a.ravel() for a in arrays]), axis)
    return tuple((running[b:e].reshape(a.shape) for a, b, e in zip(arrays, ends, ends[1:])))


def cut_along(array, dim, peers):
    dims = array.shape
    blocks = array.reshape(*dims[:dim], peers, dims[dim] // peers, *dims[dim + 1 :])
    return jnp.moveaxis(blocks, dim, 0)


def summed_on_arrival(array, axis, dim):
    blocks = cut_along(array, dim, lax.axis_size(axis))
    arrived = lax.all_to_all(blocks, axis, split_axis=0, concat_axis=0, tiled=True)
    return arrived.astype(jnp.float32).sum(axis=0)


def joined_along(blocks, dim):
    dims = list(blocks.shape[1:])
    dims[dim] *= blocks.shape[0]
    return jnp.moveaxis(blocks, 0, dim).reshape(dims)


def gathered_copies(array, axis, dim):
    return joined_along(copy_for_each(array, axis), dim)


def collect(up_weight, down_weight):
    return in_one_piece((up_weight, down_weight), "sp", 0, 1)


def attend_rows(query_rows, first_pos, keys_all, values_all, breaks_all, heads_here):
    tok_rows = query_rows.shape[0]
    head_size = query_rows.shape[1] // heads_here
    scale = head_size ** (-0.5)
    block_count = (first_pos + tok_rows + KEY_BLOCK - 1) // KEY_BLOCK
    query_heads = query_rows.reshape(tok_rows, heads_here, head_size)
    query_pos = first_pos + jnp.arange(tok_rows, dtype=jnp.int32)

    def visit(turn, carry):
        later_sum, totals = carry
        start = (block_count - 1 - turn) * KEY_BLOCK
        key_tile_rows = lax.dynamic_slice_in_dim(keys_all, start, KEY_BLOCK, 0).reshape(
            KEY_BLOCK, heads_here, head_size
        )
        value_block = lax.dynamic_slice_in_dim(values_all, start, KEY_BLOCK, 0).reshape(
            KEY_BLOCK, heads_here, head_size
        )
        break_block = lax.dynamic_slice_in_dim(breaks_all, start, KEY_BLOCK, 0).astype(jnp.float32)
        scores = (
            jnp.einsum(
                "qhd,khd->hqk", query_heads, key_tile_rows, preferred_element_type=jnp.float32
            )
            * scale
        )
        scores = scores + break_block.T[:, None, :]
        key_pos = start + jnp.arange(KEY_BLOCK, dtype=jnp.int32)
        strict = (key_pos[None, :] < query_pos[:, None])[None]
        log_break = jax.nn.log_sigmoid(scores)
        log_keep = jnp.where(strict, log_break - scores, 0.0)
        later = lax.cumsum(log_keep, axis=2, reverse=True) - log_keep + later_sum[:, :, None]
        weights = jnp.where(strict, jnp.exp(log_break + later), 0.0).astype(jnp.bfloat16)
        totals = totals + jnp.einsum(
            "hqk,khd->qhd", weights, value_block, preferred_element_type=jnp.float32
        )
        return (later_sum + jnp.sum(log_keep, axis=2), totals)

    start_state = (
        jnp.zeros((heads_here, tok_rows), jnp.float32),
        jnp.zeros((tok_rows, heads_here, head_size), jnp.float32),
    )
    totals = lax.fori_loop(0, block_count, visit, start_state)[1]
    return totals.reshape(tok_rows, heads_here * head_size).astype(jnp.bfloat16)


def attend(queries, keys, values, breaks):
    keys_all, values_all, breaks_all = in_one_piece((keys, values, breaks), "sp", 0, 1)
    tok_rows = queries.shape[0]
    heads_here = breaks.shape[1]
    offset = lax.axis_index("sp") * tok_rows
    half = tok_rows // 2
    bit_count = lax.axis_size("sp").bit_length() - 1
    mirror_offset = (lax.axis_size("sp") - 1 - lax.axis_index("sp")) * tok_rows
    early_rows = queries[:half]
    traded = queries[half:]
    for bit in range(bit_count):
        traded = from_partner(traded, "sp", bit)
    early_out = attend_rows(early_rows, offset, keys_all, values_all, breaks_all, heads_here)
    traded_out = attend_rows(
        traded, mirror_offset + half, keys_all, values_all, breaks_all, heads_here
    )
    for bit in range(bit_count):
        traded_out = from_partner(traded_out, "sp", bit)
    return jnp.concatenate([early_out, traded_out], axis=0)


def normalize(pre, gain, shift):
    row_sum, row_squares = together((jnp.sum(pre, axis=-1), jnp.sum(pre * pre, axis=-1)), "tp")
    center = row_sum / D
    spread = row_squares / D - center * center
    return (pre - center[:, None]) * lax.rsqrt(spread + EPSILON)[:, None] * gain + shift


def body(
    queries,
    keys,
    values,
    breaks,
    residual_in,
    out_weight,
    first_gain,
    first_shift,
    up_weight,
    down_weight,
    second_gain,
    second_shift,
):
    attended = attend(queries, keys, values, breaks)
    up_full, down_full = collect(up_weight, down_weight)
    columns = residual_in.shape[1]
    column_start = lax.axis_index("tp") * columns
    partial_value = jnp.dot(attended, out_weight, preferred_element_type=jnp.float32)
    mixed = summed_on_arrival(partial_value.astype(jnp.bfloat16), "tp", 1)
    pre = ALPHA * residual_in.astype(jnp.float32) + mixed
    gain_here = lax.dynamic_slice_in_dim(first_gain, column_start, columns, 0)
    shift_here = lax.dynamic_slice_in_dim(first_shift, column_start, columns, 0)
    first_out = normalize(pre, gain_here, shift_here).astype(jnp.bfloat16)
    hidden_pre = jnp.dot(
        gathered_copies(first_out, "tp", 1), up_full, preferred_element_type=jnp.float32
    )
    activated = jnp.square(jax.nn.relu(hidden_pre)).astype(jnp.bfloat16)
    hidden_partial = lax.dot_general(
        activated, down_full, (((1,), (1,)), ((), ())), preferred_element_type=jnp.float32
    )
    channel_mix = summed_on_arrival(hidden_partial.astype(jnp.bfloat16), "tp", 1)
    second_pre = ALPHA * first_out.astype(jnp.float32) + channel_mix
    gain_second = lax.dynamic_slice_in_dim(second_gain, column_start, columns, 0)
    shift_second = lax.dynamic_slice_in_dim(second_shift, column_start, columns, 0)
    return normalize(second_pre, gain_second, shift_second).astype(jnp.bfloat16)


def solution(mesh):
    return jax.shard_map(
        body,
        mesh=mesh,
        in_specs=(
            P("sp", "tp"),
            P("sp", "tp"),
            P("sp", "tp"),
            P("sp", "tp"),
            P("sp", "tp"),
            P("tp", None),
            P(),
            P(),
            P("sp", "tp"),
            P("sp", "tp"),
            P(),
            P(),
        ),
        out_specs=P("sp", "tp"),
        check_vma=False,
    )
```

profile of v0, /device:TPU:120, one launch (start us, length us, event | category | flops | bytes accessed | tf_op | source)
XLA Modules:
  0.0 571.9 jit_solution(1776094923094058598)
XLA Ops:
  11.0 3.5 collective-permute-done
  15.8 4.5 collective-permute-done.1
  20.4 4.2 collective-permute-done.2
  26.3 5.4 collective-permute-done.3
  31.7 5.0 collective-permute-start.4
  36.7 92.5 %all-gather.3.cloned.1.call-done = bf16[16384,257]{1,0:T(8,128)(2,1)} async-done(((bf16[512,257]{1,0:T(8,128)(2,1)}), bf16[16384,257]{1,0:T(8,128)(2,1)}) %all-gather.3.cloned.1.call-update) | async-done | bytes 8421392 | tf_op jit(solution)/shard_map/all_gather | solution.py:20
  129.1 5.8 %fusion.57 = (bf16[16384,128]{1,0:T(8,128)(2,1)}, bf16[16384,128]{1,0:T(8,128)(2,1)}) fusion(bf16[16384,257]{1,0:T(8,128)(2,1)} %all-gather.3.cloned.1.call-done), kind=kLoop, calls=%fused_computation.94 | loop fusion | bytes 16777216 | tf_op jit(solution)/shard_map/split | solution.py:20
  134.9 3.7 split.21
  138.6 3.7 copy.53
  142.4 97.5 %while.31 = (s32[]{:T(128)}, f32[1,256]{1,0:T(1,128)S(1)}, f32[256,1,128]{0,2,1:T(8,128)S(1)}, s32[]{:T(128)}, s32[]{:T(128)}, /*index=5*/bf16[16384,128]{1,0:T(...) while((s32[]{:T(128)}, f32[1,256]{1,0:T(1,128)S(1)}, ...), condition=%wide.region_9.10_spmd.clone, body=%wide.region_5.9_spmd.clone.sunk | while | flops 87593992 | bytes 5882079 | solution.py:113
  239.9 7.0 %collective-permute-start.5 = (bf16[256,128]{0,1:T(8,128)(2,1)S(1)}, bf16[256,128]{0,1:T(8,128)(2,1)S(1)}, u32[]{:S(2)}, u32[]{:S(2)}) collective-permute-start(bf16[256,128]{0,1:T(8,128)(2,1)S(1)} %convert_bitcast_fusion), channel_id=1, source_target_pairs={{0,8},{8,0},{16,24},{24,16},{32,40},{40,32},{48,56},{56,48},{64,72... | collective-permute-start | bytes 196616 | tf_op jit(solution)/shard_map/ppermute | solution.py:24
  249.2 14.1 %collective-permute-start.6 = (bf16[256,128]{0,1:T(8,128)(2,1)S(1)}, bf16[256,128]{0,1:T(8,128)(2,1)S(1)}, u32[]{:S(2)}, u32[]{:S(2)}) collective-permute-start(bf16[256,128]{0,1:T(8,128)(2,1)S(1)} %collective-permute-done.5), channel_id=1, source_target_pairs={{0,16},{8,24},{16,0},{24,8},{32,48},{40,56},{48,32},{56,40},{64,80... | collective-permute-start | bytes 196616 | tf_op jit(solution)/shard_map/ppermute | solution.py:24
  265.6 22.2 %collective-permute-start.7 = (bf16[256,128]{0,1:T(8,128)(2,1)S(1)}, bf16[256,128]{0,1:T(8,128)(2,1)S(1)}, u32[]{:S(2)}, u32[]{:S(2)}) collective-permute-start(bf16[256,128]{0,1:T(8,128)(2,1)S(1)} %collective-permute-done.6), channel_id=1, source_target_pairs={{0,32},{8,40},{16,48},{24,56},{32,0},{40,8},{48,16},{56,24},{64,96... | collective-permute-start | bytes 196616 | tf_op jit(solution)/shard_map/ppermute | solution.py:24
  290.0 48.4 %collective-permute-start.8 = (bf16[256,128]{0,1:T(8,128)(2,1)S(1)}, bf16[256,128]{0,1:T(8,128)(2,1)S(1)}, u32[]{:S(2)}, u32[]{:S(2)}) collective-permute-start(bf16[256,128]{0,1:T(8,128)(2,1)S(1)} %collective-permute-done.7), channel_id=1, source_target_pairs={{0,64},{8,72},{16,80},{24,88},{32,96},{40,104},{48,112},{56,120},{... | collective-permute-start | bytes 196616 | tf_op jit(solution)/shard_map/ppermute | solution.py:24
  338.4 91.9 %while.30 = (s32[]{:T(128)}, f32[1,256]{1,0:T(1,128)S(1)}, f32[256,1,128]{0,2,1:T(8,128)S(1)}, s32[]{:T(128)}, s32[]{:T(128)}, /*index=5*/bf16[16384,128]{1,0:T(...) while((s32[]{:T(128)}, f32[1,256]{1,0:T(1,128)S(1)}, ...), condition=%wide.region_4.5_spmd.clone, body=%wide.region_0.4_spmd.clone.sunk | while | flops 87593992 | bytes 5882079 | solution.py:113
  433.6 5.0 collective-permute-done.9
  439.5 31.4 %all_to_all.27 = bf16[8,512,256]{2,1,0:T(8,128)(2,1)S(1)} all-to-all(bf16[8,512,256]{2,1,0:T(8,128)(2,1)S(1)} %bitcast.145), channel_id=1, replica_groups=mesh['sp'=32,'tp'=8] {'tp'}, dimensions={0} | all-to-all | bytes 4194304 | tf_op jit(solution)/shard_map/all_to_all | solution.py:55
  477.0 3.8 all-to-all-done.1
  482.7 3.6 all-to-all-start.2
  486.4 27.1 %all-to-all-done.2 = bf16[8,512,256]{1,2,0:T(8,128)(2,1)S(1)} async-done(((bf16[8,512,256]{1,2,0:T(8,128)(2,1)}), bf16[8,512,256]{1,2,0:T(8,128)(2,1)S(1)}, u32[]{:S(2)}, u32[]{:S(2)}) %all-to-all-start.2) | async-done | bytes 2097184 | tf_op jit(solution)/shard_map/all_to_all | solution.py:29
  513.4 9.3 %fusion.40 = bf16[512,2048]{1,0:T(8,128)(2,1)} fusion(bf16[2048,2048]{1,0:T(8,128)(2,1)} %all-gather.5.cloned.1.call-done, bf16[512,2048]{0,1:T(8,128)(2,1)S(1)} %bitcast.147), kind=kOutput, calls=%fused_computation.62 | convolution fusion | flops 4297588736 | bytes 12582912 | tf_op jit(solution)/shard_map/dot_general | solution.py:173
  524.5 29.7 %all_to_all.28 = bf16[8,512,256]{2,1,0:T(8,128)(2,1)S(1)} all-to-all(bf16[8,512,256]{2,1,0:T(8,128)(2,1)S(1)} %bitcast.146), channel_id=1, replica_groups=mesh['sp'=32,'tp'=8] {'tp'}, dimensions={0} | all-to-all | bytes 4194304 | tf_op jit(solution)/shard_map/all_to_all | solution.py:55
  555.3 3.3 all-to-all-start.4
  560.2 3.8 all-to-all-done.4
  (449 shorter events, 218.1 us)
Async XLA Ops:
  6.5 432.1 %copy-start = (bf16[128,2048]{1,0:T(8,128)(2,1)S(1)}, bf16[128,2048]{1,0:T(8,128)(2,1)}, u32[]{:S(2)}) copy-start(bf16[128,2048]{1,0:T(8,128)(2,1)} %param.21) | copy-start | bytes 1572868
  6.5 122.6 %all-gather.3.cloned.1.call-start = ((), (), s32[]{:S(2)}) async-start(), calls=%async_computation.5 | async-start | bytes 12976128 | tf_op jit(solution)/shard_map/all_gather | solution.py:20
  9.3 477.1 %all-gather.5.cloned.1.call-start = ((), (), s32[]{:S(2)}) async-start(), calls=%async_computation.6 | async-start | bytes 8650752 | tf_op jit(solution)/shard_map/all_gather | solution.py:20
  10.2 4.4 collective-permute-start
  14.5 5.8 %collective-permute-start.1 = (bf16[256,128]{1,0:T(8,128)(2,1)S(1)}, bf16[256,128]{1,0:T(8,128)(2,1)S(1)}, u32[]{:S(2)}, u32[]{:S(2)}) collective-permute-start(bf16[256,128]{1,0:T(8,128)(2,1)S(1)} %collective-permute-done), channel_id=1, source_target_pairs={{0,16},{8,24},{16,0},{24,8},{32,48},{40,56},{48,32},{56,40},{64,80... | collective-permute-start | bytes 196616 | tf_op jit(solution)/shard_map/ppermute | solution.py:24
  20.3 4.3 collective-permute-start.2
  24.6 7.1 %collective-permute-start.3 = (bf16[256,128]{1,0:T(8,128)(2,1)S(1)}, bf16[256,128]{1,0:T(8,128)(2,1)S(1)}, u32[]{:S(2)}, u32[]{:S(2)}) collective-permute-start(bf16[256,128]{1,0:T(8,128)(2,1)S(1)} %collective-permute-done.2), channel_id=1, source_target_pairs={{0,64},{8,72},{16,80},{24,88},{32,96},{40,104},{48,112},{56,120},{... | collective-permute-start | bytes 196616 | tf_op jit(solution)/shard_map/ppermute | solution.py:24
  31.7 110.6 %collective-permute-start.4 = (bf16[256,128]{1,0:T(8,128)(2,1)S(1)}, bf16[256,128]{1,0:T(8,128)(2,1)S(1)}, u32[]{:S(2)}, u32[]{:S(2)}) collective-permute-start(bf16[256,128]{1,0:T(8,128)(2,1)S(1)} %collective-permute-done.3), channel_id=1, source_target_pairs={{0,128},{8,136},{16,144},{24,152},{32,160},{40,168},{48,176},{56,1... | collective-permute-start | bytes 196616 | tf_op jit(solution)/shard_map/ppermute | solution.py:24
  239.9 9.2 %collective-permute-start.5 = (bf16[256,128]{0,1:T(8,128)(2,1)S(1)}, bf16[256,128]{0,1:T(8,128)(2,1)S(1)}, u32[]{:S(2)}, u32[]{:S(2)}) collective-permute-start(bf16[256,128]{0,1:T(8,128)(2,1)S(1)} %convert_bitcast_fusion), channel_id=1, source_target_pairs={{0,8},{8,0},{16,24},{24,16},{32,40},{40,32},{48,56},{56,48},{64,72... | collective-permute-start | bytes 196616 | tf_op jit(solution)/shard_map/ppermute | solution.py:24
  249.2 16.4 %collective-permute-start.6 = (bf16[256,128]{0,1:T(8,128)(2,1)S(1)}, bf16[256,128]{0,1:T(8,128)(2,1)S(1)}, u32[]{:S(2)}, u32[]{:S(2)}) collective-permute-start(bf16[256,128]{0,1:T(8,128)(2,1)S(1)} %collective-permute-done.5), channel_id=1, source_target_pairs={{0,16},{8,24},{16,0},{24,8},{32,48},{40,56},{48,32},{56,40},{64,80... | collective-permute-start | bytes 196616 | tf_op jit(solution)/shard_map/ppermute | solution.py:24
  265.6 24.4 %collective-permute-start.7 = (bf16[256,128]{0,1:T(8,128)(2,1)S(1)}, bf16[256,128]{0,1:T(8,128)(2,1)S(1)}, u32[]{:S(2)}, u32[]{:S(2)}) collective-permute-start(bf16[256,128]{0,1:T(8,128)(2,1)S(1)} %collective-permute-done.6), channel_id=1, source_target_pairs={{0,32},{8,40},{16,48},{24,56},{32,0},{40,8},{48,16},{56,24},{64,96... | collective-permute-start | bytes 196616 | tf_op jit(solution)/shard_map/ppermute | solution.py:24
  290.0 140.4 %collective-permute-start.8 = (bf16[256,128]{0,1:T(8,128)(2,1)S(1)}, bf16[256,128]{0,1:T(8,128)(2,1)S(1)}, u32[]{:S(2)}, u32[]{:S(2)}) collective-permute-start(bf16[256,128]{0,1:T(8,128)(2,1)S(1)} %collective-permute-done.7), channel_id=1, source_target_pairs={{0,64},{8,72},{16,80},{24,88},{32,96},{40,104},{48,112},{56,120},{... | collective-permute-start | bytes 196616 | tf_op jit(solution)/shard_map/ppermute | solution.py:24
  430.4 8.3 %collective-permute-start.9 = (bf16[256,128]{0,1:T(8,128)(2,1)S(1)}, bf16[256,128]{0,1:T(8,128)(2,1)S(1)}, u32[]{:S(2)}, u32[]{:S(2)}) collective-permute-start(bf16[256,128]{0,1:T(8,128)(2,1)S(1)} %collective-permute-done.8), channel_id=1, source_target_pairs={{0,128},{8,136},{16,144},{24,152},{32,160},{40,168},{48,176},{56,1... | collective-permute-start | bytes 196616 | tf_op jit(solution)/shard_map/ppermute | solution.py:24
  439.5 31.7 %copy-start.1 = (bf16[512,256]{1,0:T(8,128)(2,1)S(1)}, bf16[512,256]{1,0:T(8,128)(2,1)}, u32[]{:S(2)}) copy-start(bf16[512,256]{1,0:T(8,128)(2,1)} %param.20) | copy-start | bytes 786436
  472.1 8.7 %all-to-all-start.1 = ((f32[8,1,1024]{2,1,0:T(1,128)}), f32[8,1,1024]{2,1,0:T(1,128)S(1)}, u32[]{:S(2)}, u32[]{:S(2)}) async-start(f32[8,1,1024]{2,1,0:T(1,128)} %broadcast_in_dim.19), calls=%async_computation.1 | async-start | bytes 65536 | tf_op jit(solution)/shard_map/all_to_all | solution.py:29
  482.7 30.7 %all-to-all-start.2 = ((bf16[8,512,256]{1,2,0:T(8,128)(2,1)}), bf16[8,512,256]{1,2,0:T(8,128)(2,1)S(1)}, u32[]{:S(2)}, u32[]{:S(2)}) async-start(bf16[8,512,256]{1,2,0:T(8,128)(2,1)} %broadcast_in_dim.20), calls=%async_computation.2 | async-start | bytes 4194304 | tf_op jit(solution)/shard_map/all_to_all | solution.py:29
  555.3 8.7 %all-to-all-start.4 = ((f32[8,1,1024]{2,1,0:T(1,128)}), f32[8,1,1024]{2,1,0:T(1,128)S(1)}, u32[]{:S(2)}, u32[]{:S(2)}) async-start(f32[8,1,1024]{2,1,0:T(1,128)} %broadcast_in_dim.21), calls=%async_computation.4 | async-start | bytes 65536 | tf_op jit(solution)/shard_map/all_to_all | solution.py:29
Sparse Core Ops, SparseCore 0:
  9.9 119.1 all-gather.2
  131.7 95.2 all-gather.4
where the time goes:
time: 574 us; the launch traced here: 572 us
  waiting for transfers between devices  157 us (27%)
  starting transfers between devices  112 us (20%)
  other arithmetic  101 us (18%)
  matrix products  97.3 us (17%)
  blocking collectives  61.1 us (11%)
  local copies, waits for them, and re-layouts  26.6 us (5%)
  between operations  13.6 us (2%)
    ppermute x10, starting transfers between devices, from_partner(): lax.ppermute(array, axis, [(i, i ^ 1 << distance) for i in range(lax.axis...  102 us
    all_gather x2, waiting for transfers between devices, in_one_piece(): lax.all_gather(both, axis, axis=dim, tiled=True)  92.5 us
    another operation x66, other arithmetic  79.1 us
    all_to_all x2, blocking collectives, summed_on_arrival(): lax.all_to_all(blocks, axis, split_axis=0, concat_axis=0, tiled=True)  61.1 us
    dot_general x33, matrix products, visit(): jnp.einsum('qhd,khd->hqk', query_heads, key_tile_rows, preferred_element_...  49.4 us
    dot_general x33, matrix products, visit(): jnp.einsum('hqk,khd->qhd', weights, value_block, preferred_element_type=j...  37.8 us
    all_to_all x3, waiting for transfers between devices, copy_for_each(): lax.all_to_all(jnp.broadcast_to(array[None], (peers, *array.shape)), axis...  34.7 us
    ppermute x10, waiting for transfers between devices, from_partner(): lax.ppermute(array, axis, [(i, i ^ 1 << distance) for i in range(lax.axis...  29.3 us
  transfers between devices with their start and end apart: 15, of which 12 were waited for; matrix products, arithmetic and copies ran while one was open for 37% of the time, Pallas kernels for 0%

commit v1 on v0

v1 whole, which is shorter than its diff:
```python
import functools
import math

import jax
import jax.numpy as jnp
from jax import lax
from jax.experimental import pallas as pl
from jax.experimental.pallas import tpu as pltpu
from jax.sharding import PartitionSpec as P

MESH = pl.DeviceIdType.MESH
ALPHA = 2.0**0.25
EPSILON = 1e-05
LOG2E = math.log2(math.e)
CLAMP = 120.0
F32 = jnp.float32
BF16 = jnp.bfloat16
NT = (((1,), (1,)), ((), ()))


def split_sp(n_sp):
    ny = 4 if n_sp == 32 else 2
    return n_sp // ny, ny


def iota(shape, dim):
    return lax.broadcasted_iota(jnp.int32, shape, dim)


class Mail:
    def __init__(self, send, recv):
        self.send, self.recv = send, recv

    def make(self, m, src, dst, target):
        return pltpu.make_async_remote_copy(
            src_ref=src,
            dst_ref=dst,
            send_sem=self.send.at[m],
            recv_sem=self.recv.at[m],
            device_id=target,
            device_id_type=MESH,
        )

    def start(self, m, src, dst, target):
        self.make(m, src, dst, target).start()

    def arrived(self, m, dst, target):
        self.make(m, dst, dst, target).wait_recv()

    def sent(self, m, src, target):
        self.make(m, src, src, target).wait_send()


class Gather:
    def __init__(self, mail, base, slot, nx):
        self.mail, self.base, self.slot, self.nx = mail, base, slot, nx
        me = lax.axis_index("tp")
        self.me, self.x, self.c = me, me // 2, me % 2
        self.sib = {"tp": self.x * 2 + 1 - self.c}

    @staticmethod
    def count(nx):
        return 2 * nx

    def at(self, r, core):
        return lax.rem(self.x + self.nx + r, self.nx) * 2 + core

    def start(self, src):
        for r in range(1, self.nx):
            self.mail.start(self.base + r, src, self.slot(self.me), {"tp": self.at(r, self.c)})
        self.mail.start(self.base, src, self.slot(self.me), self.sib)

    def forward(self):
        for r in range(1, self.nx):
            got = self.slot(self.at(-r, self.c))
            self.mail.arrived(self.base + r, got, self.sib)
            self.mail.start(self.base + self.nx + r, got, got, self.sib)

    def finish(self):
        other = 1 - self.c
        self.mail.arrived(self.base, self.slot(self.at(0, other)), self.sib)
        for r in range(1, self.nx):
            self.mail.arrived(self.base + self.nx + r, self.slot(self.at(-r, other)), self.sib)

    def drain(self):
        for r in range(self.nx):
            self.mail.sent(self.base + r, self.slot(self.me), self.sib)
        for r in range(1, self.nx):
            self.mail.sent(self.base + self.nx + r, self.slot(self.me), self.sib)


def attention_kernel(
    nz, ny, nx,
    q_ref, k_ref, v_ref, b_ref, ow_ref, res_ref, gain_ref, shift_ref,
    fo_ref,
    qbuf, kb, vb, bb, tri, pacc, tcol, tt, fac, part, partf, prec, stage,
    ow_full, res_full, att_full, pre,
    msend, mrecv, ksend, krecv, vsend, vrecv,
):
    sp = lax.axis_index("sp")
    z, y = sp // ny, lax.rem(sp, ny)
    me = lax.axis_index("tp")
    tb, hd = k_ref.shape
    half = tb // 2
    rows = 2 * ny * half
    mail = Mail(msend, mrecv)
    kmail, vmail = Mail(ksend, krecv), Mail(vsend, vrecv)

    def zdev(zz):
        return {"sp": zz * ny + y}

    def ydev(r):
        return {"sp": z * ny + lax.rem(y + ny + r, ny)}

    mirror = zdev(nz - 1 - z)

    barrier = pltpu.get_barrier_semaphore()
    for r in range(1, nz):
        pl.semaphore_signal(barrier, inc=1, device_id=zdev(lax.rem(z + r, nz)), device_id_type=MESH)
    for r in range(1, ny):
        pl.semaphore_signal(barrier, inc=1, device_id=ydev(r), device_id_type=MESH)
    for r in range(1, 2 * nx):
        pl.semaphore_signal(
            barrier, inc=1, device_id={"tp": lax.rem(me + r, 2 * nx)}, device_id_type=MESH
        )
    pl.semaphore_wait(barrier, nz - 1 + ny - 1 + 2 * nx - 1)

    m_q1, m_q2, m_q2f = 0, ny, 2 * ny
    m_b = 3 * ny
    m_t = m_b + nz
    m_p = m_t + ny
    m_ret = m_p + ny
    g0 = m_ret + 1
    gn = Gather.count(nx)
    g_ow = Gather(mail, g0, lambda j: ow_full.at[pl.ds(j * hd, hd), :], nx)
    dw = res_ref.shape[1]
    g_res = Gather(
        mail, g0 + gn, lambda j: res_full.at[:, pl.ds(pl.multiple_of(j * dw, dw), dw)], nx
    )
    g_att = [
        Gather(
            mail,
            g0 + (2 + h) * gn,
            functools.partial(
                lambda h, j: att_full.at[pl.ds(h * half, half), pl.ds(pl.multiple_of(j * hd, hd), hd)], h
            ),
            nx,
        )
        for h in range(2)
    ]

    early, late = q_ref.at[pl.ds(0, half), :], q_ref.at[pl.ds(half, half), :]
    mail.start(m_q2, late, qbuf.at[ny + y], mirror)
    for r in range(1, ny):
        mail.start(m_q1 + r, early, qbuf.at[y], ydev(r))
    for r in range(1, nz):
        mail.start(m_b + r, b_ref, bb.at[z], zdev(lax.rem(z + r, nz)))
    right, left = zdev(lax.rem(z + 1, nz)), zdev(lax.rem(z + nz - 1, nz))
    kmail.start(1, k_ref, kb.at[1], right)
    kmail.start(2, k_ref, kb.at[2], left)
    vmail.start(1, v_ref, vb.at[1], right)
    vmail.start(2, v_ref, vb.at[2], left)
    g_ow.start(ow_ref)
    g_res.start(res_ref)

    qbuf[y] = q_ref[:half, :]
    bb[z] = b_ref[...]
    kb[0] = k_ref[...]
    vb[0] = v_ref[...]
    ow_full[pl.ds(me * hd, hd), :] = ow_ref[...]
    res_full[:, pl.ds(pl.multiple_of(me * dw, dw), dw)] = res_ref[...]
    tri[...] = (iota((tb, tb), 0) > iota((tb, tb), 1)).astype(BF16)
    tcol[...] = jnp.zeros_like(tcol)
    fac[...] = jnp.zeros_like(fac)

    mail.arrived(m_q2, qbuf.at[ny + y], mirror)
    for r in range(1, ny):
        mail.start(m_q2f + r, qbuf.at[ny + y], qbuf.at[ny + y], ydev(r))
    for r in range(1, ny):
        mail.arrived(m_q1 + r, qbuf.at[lax.rem(y + ny - r, ny)], ydev(r))
    for r in range(1, ny):
        mail.arrived(m_q2f + r, qbuf.at[ny + lax.rem(y + ny - r, ny)], ydev(r))
    for r in range(1, nz):
        mail.arrived(m_b + r, bb.at[lax.rem(z + nz - r, nz)], left)

    scale = hd ** (-0.5) * LOG2E
    hk = tb // 2
    lane = iota((half, 128), 1)

    @pl.loop(0, nz)
    def _(i):
        odd = lax.rem(i, 2)
        step = (i + 1) // 2
        zb = lax.rem(jnp.where(odd == 1, z - step, z + step) + nz, nz)
        onward = zdev(lax.rem(jnp.where(odd == 1, z + 1, z - 1) + nz, nz))

        @pl.when(i > 0)
        def _():
            kmail.arrived(i, kb.at[i], onward)
            vmail.arrived(i, vb.at[i], onward)

        @pl.when(jnp.logical_and(i >= 1, i <= nz - 4))
        def _():
            kmail.start(i + 2, kb.at[i], kb.at[i + 2], onward)
            vmail.start(i + 2, vb.at[i], vb.at[i + 2], onward)

        @pl.when(i == nz - 3)
        def _():
            kmail.start(nz - 1, kb.at[i], kb.at[nz - 1], onward)

        @pl.when(i == nz - 2)
        def _():
            vmail.start(nz - 1, vb.at[i], vb.at[nz - 1], onward)

        def tile(t, h, masked):
            where = pl.ds(pl.multiple_of(t * half, half), half)
            scores = lax.dot_general(qbuf[t], kb[i], NT, preferred_element_type=F32)
            logits = scores * scale + bb[zb][0:1, :]
            soft = jnp.maximum(
                jnp.log(1.0 + jnp.exp2(jnp.minimum(logits, CLAMP))) * LOG2E, logits
            )
            brk = logits - soft
            if masked:
                strict = iota((half, tb), 1) < iota((half, tb), 0) + h * half
                soft = jnp.where(strict, soft, 0.0)
            soft16 = soft.astype(BF16)
            later0 = jnp.dot(soft16, tri[:, :hk], preferred_element_type=F32)
            later1 = jnp.dot(soft16[:, hk:], tri[hk:, hk:], preferred_element_type=F32)
            w0 = jnp.exp2(brk[:, :hk] - later0)
            w1 = jnp.exp2(brk[:, hk:] - later1)
            if masked:
                w0 = jnp.where(strict[:, :hk], w0, 0.0)
                w1 = jnp.where(strict[:, hk:], w1, 0.0)
            pacc[zb, where, :] = jnp.dot(
                w0.astype(BF16), vb[i, :hk, :], preferred_element_type=F32
            ) + jnp.dot(w1.astype(BF16), vb[i, hk:, :], preferred_element_type=F32)
            total = later0[:, 0:1] + soft[:, 0:1]
            tcol[where, :] = jnp.where(lane == zb, total, tcol[where, :])

        @pl.loop(0, 2 * ny)
        def _(t):
            h = t // ny
            qz = jnp.where(h == 0, z, nz - 1 - z)
            qblock = qz * ny + lax.rem(t, ny)
            kblock = zb * ny + y

            @pl.when(kblock < qblock)
            def _():
                tile(t, h, False)

            @pl.when(kblock == qblock)
            def _():
                tile(t, h, True)

            @pl.when(kblock > qblock)
            def _():
                where = pl.ds(pl.multiple_of(t * half, half), half)
                pacc[zb, where, :] = jnp.zeros((half, hd), F32)

    @pl.loop(0, rows // 128)
    def _(n):
        at = pl.ds(pl.multiple_of(n * 128, 128), 128)
        tt[y, :, at] = tcol[at, :].T[:8, :]

    for r in range(1, ny):
        mail.start(m_t + r, tt.at[y], tt.at[y], ydev(r))
    g_ow.forward()
    g_res.forward()
    for r in range(1, ny):
        mail.arrived(m_t + r, tt.at[lax.rem(y + ny - r, ny)], ydev(r))
    every = tt[0]
    after = jnp.zeros_like(every)
    for yy in range(ny):
        if yy:
            every = every + tt[yy]
        after = after + jnp.where(yy > y, tt[yy], 0.0)
    beyond = jnp.zeros_like(every[0:1, :])
    for zz in reversed(range(nz)):
        fac[zz : zz + 1, :] = jnp.exp2(-(beyond + after[zz : zz + 1, :]))
        beyond = beyond + every[zz : zz + 1, :]

    chunk = min(128, half)
    per = half // chunk

    @pl.loop(0, rows // 128)
    def _(n):
        at = pl.ds(pl.multiple_of(n * 128, 128), 128)
        cols = fac[:, at].T
        acc = cols[:, 0:1] * pacc[0, at, :]
        for zz in range(1, nz):
            acc = acc + cols[:, zz : zz + 1] * pacc[zz, at, :]
        partf[at, :] = acc
        part[at, :] = acc.astype(BF16)

    for r in range(1, ny):
        for h in range(2):
            to = lax.rem(y + r, ny)
            src = part.at[pl.ds(pl.multiple_of((h * ny + to) * half, half), half), :]
            mail.start(m_p + r if h == 0 else m_p2(m_p, r, g0, gn), src, prec.at[y, h], ydev(r))
    own = lambda h: partf[pl.ds(pl.multiple_of((h * ny + y) * half, half), half), :]

    def summed(h):
        acc = own(h)
        for r in range(1, ny):
            frm = lax.rem(y + ny - r, ny)
            mail.arrived(m_p + r if h == 0 else m_p2(m_p, r, g0, gn), prec.at[frm, h], ydev(r))
            acc = acc + prec[frm, h].astype(F32)
        return acc.astype(BF16)

    mycol = pl.ds(pl.multiple_of(me * hd, hd), hd)
    stage[...] = summed(1)
    mail.start(m_ret, stage, att_full.at[pl.ds(half, half), mycol], mirror)
    att_full[:half, mycol] = summed(0)
    g_att[0].start(att_full.at[pl.ds(0, half), mycol])
    mail.arrived(m_ret, att_full.at[pl.ds(half, half), mycol], mirror)
    g_att[1].start(att_full.at[pl.ds(half, half), mycol])
    g_ow.finish()
    g_res.finish()
    g_att[0].forward()
    g_att[1].forward()
    g_att[0].finish()
    g_att[1].finish()

    width = ow_full.shape[1]
    nc = min(256, width)

    @pl.loop(0, width // nc)
    def _(n):
        at = pl.ds(pl.multiple_of(n * nc, nc), nc)
        pre[:, at] = jnp.dot(att_full[...], ow_full[:, at], preferred_element_type=F32) + (
            ALPHA * res_full[:, at].astype(F32)
        )

    rc = 64

    @pl.loop(0, tb // rc)
    def _(n):
        at = pl.ds(pl.multiple_of(n * rc, rc), rc)
        row = pre[at, :]
        center = jnp.mean(row, axis=-1, keepdims=True)
        off = row - center
        spread = jnp.mean(off * off, axis=-1, keepdims=True)
        fo_ref[at, :] = (off * lax.rsqrt(spread + EPSILON) * gain_ref[...] + shift_ref[...]).astype(
            BF16
        )

    mail.sent(m_q2, late, mirror)
    for r in range(1, ny):
        mail.sent(m_q1 + r, early, mirror)
        mail.sent(m_q2f + r, early, mirror)
        mail.sent(m_t + r, tt.at[y], mirror)
        mail.sent(m_p + r, stage, mirror)
        mail.sent(m_p2(m_p, r, g0, gn), stage, mirror)
    for r in range(1, nz):
        mail.sent(m_b + r, b_ref, mirror)
    mail.sent(m_ret, stage, mirror)

    @pl.loop(1, nz)
    def _(i):
        kmail.sent(i, kb.at[0], mirror)
        vmail.sent(i, vb.at[0], mirror)

    for g in [g_ow, g_res] + g_att:
        g.drain()


def m_p2(m_p, r, g0, gn):
    return g0 + 4 * gn + r


def attention_layer(nz, ny, nx, q, k, v, bias, ow, res, gain, shift):
    tb, hd = q.shape
    half = tb // 2
    rows = 2 * ny * half
    width = ow.shape[1]
    ntp = 2 * nx
    gn = Gather.count(nx)
    messages = 3 * ny + nz + 2 * ny + 1 + 4 * gn + ny
    vm = pl.BlockSpec(memory_space=pltpu.VMEM)
    dma = pltpu.SemaphoreType.DMA
    return pl.pallas_call(
        functools.partial(attention_kernel, nz, ny, nx),
        out_shape=jax.ShapeDtypeStruct((tb, width), BF16),
        in_specs=[vm] * 8,
        out_specs=vm,
        scratch_shapes=[
            pltpu.VMEM((2 * ny, half, hd), BF16),
            pltpu.VMEM((nz, tb, hd), BF16),
            pltpu.VMEM((nz, tb, hd), BF16),
            pltpu.VMEM((nz, 8, tb), F32),
            pltpu.VMEM((tb, tb), BF16),
            pltpu.VMEM((nz, rows, hd), F32),
            pltpu.VMEM((rows, 128), F32),
            pltpu.VMEM((ny, 8, rows), F32),
            pltpu.VMEM((128, rows), F32),
            pltpu.VMEM((rows, hd), BF16),
            pltpu.VMEM((rows, hd), F32),
            pltpu.VMEM((ny, 2, half, hd), BF16),
            pltpu.VMEM((half, hd), BF16),
            pltpu.VMEM((ntp * hd, width), BF16),
            pltpu.VMEM((tb, width), BF16),
            pltpu.VMEM((tb, ntp * hd), BF16),
            pltpu.VMEM((tb, width), F32),
            dma((messages,)),
            dma((messages,)),
            dma((nz,)),
            dma((nz,)),
            dma((nz,)),
            dma((nz,)),
        ],
        compiler_params=pltpu.CompilerParams(
            collective_id=0, has_side_effects=True, vmem_limit_bytes=56 * 1024 * 1024
        ),
        cost_estimate=pl.CostEstimate(flops=20_000_000_000, bytes_accessed=8_000_000, transcendentals=0),
        name="attention_layer",
    )(q, k, v, bias, ow, res, gain, shift)


def up_kernel(x_ref, w_ref, o_ref):
    hidden = jnp.maximum(jnp.dot(x_ref[...], w_ref[...], preferred_element_type=F32), 0.0)
    o_ref[...] = (hidden * hidden).astype(BF16)


def up_project(x, w):
    tb, d = x.shape
    n = w.shape[1]
    nb = min(256, n)
    return pl.pallas_call(
        up_kernel,
        out_shape=jax.ShapeDtypeStruct((tb, n), BF16),
        grid=(n // nb,),
        in_specs=[
            pl.BlockSpec((tb, d), lambda i: (0, 0)),
            pl.BlockSpec((d, nb), lambda i: (0, i)),
        ],
        out_specs=pl.BlockSpec((tb, nb), lambda i: (0, i)),
        compiler_params=pltpu.CompilerParams(vmem_limit_bytes=24 * 1024 * 1024),
        cost_estimate=pl.CostEstimate(
            flops=2 * tb * d * n, bytes_accessed=2 * (tb * d + d * n + tb * n), transcendentals=0
        ),
        name="up_project",
    )(x, w)


def down_kernel(
    nx,
    act_ref, dw_ref, fo_ref, gain_ref, shift_ref,
    out_ref,
    sbuf, sib, xbuf, rbuf, mine, cols, stat,
    ssend, srecv, xsend, xrecv, tsend, trecv,
):
    me = lax.axis_index("tp")
    x, c = me // 2, lax.rem(me, 2)
    ntp = 2 * nx
    tb, dw = out_ref.shape
    smail, xmail, tmail = Mail(ssend, srecv), Mail(xsend, xrecv), Mail(tsend, trecv)
    sibling = {"tp": x * 2 + 1 - c}

    barrier = pltpu.get_barrier_semaphore()
    for r in range(1, ntp):
        pl.semaphore_signal(
            barrier, inc=1, device_id={"tp": lax.rem(me + r, ntp)}, device_id_type=MESH
        )
    pl.semaphore_wait(barrier, ntp - 1)

    @pl.loop(0, ntp)
    def _(i):
        first = i < nx
        n = lax.rem(i, nx)
        chip = lax.rem(x + 1 + n, nx)
        j = chip * 2 + jnp.where(first, 1 - c, c)
        piece = lax.dot_general(
            act_ref[...],
            dw_ref[pl.ds(pl.multiple_of(j * dw, dw), dw), :],
            NT,
            preferred_element_type=F32,
        )

        @pl.when(first)
        def _():
            sbuf[n] = piece.astype(BF16)
            smail.start(n, sbuf.at[n], sib.at[n], sibling)

        @pl.when(jnp.logical_not(first))
        def _():
            smail.arrived(n, sib.at[n], sibling)
            both = piece + sib[n].astype(F32)

            @pl.when(n < nx - 1)
            def _():
                xbuf[n] = both.astype(BF16)
                xmail.start(n, xbuf.at[n], rbuf.at[n], {"tp": j})

            @pl.when(n == nx - 1)
            def _():
                mine[...] = both

    at = pl.ds(pl.multiple_of(me * dw, dw), dw)
    total = mine[...] + ALPHA * fo_ref[:, at].astype(F32)
    for n in range(nx - 1):
        xmail.arrived(n, rbuf.at[n], sibling)
        total = total + rbuf[n].astype(F32)
    mine[...] = total
    row_sum = jnp.sum(total, axis=-1, keepdims=True)
    row_squares = jnp.sum(total * total, axis=-1, keepdims=True)
    lane = iota((tb, 128), 1)
    cols[...] = jnp.where(lane == 0, row_sum, jnp.where(lane == 1, row_squares, 0.0))
    for n in range(tb // 128):
        stat[me, :, n * 128 : (n + 1) * 128] = cols[n * 128 : (n + 1) * 128, :].T[:8, :]
    for r in range(1, ntp):
        tmail.start(r, stat.at[me], stat.at[me], {"tp": lax.rem(me + r, ntp)})
    for r in range(1, ntp):
        tmail.arrived(r, stat.at[lax.rem(me + ntp - r, ntp)], sibling)
    sums = stat[0]
    for j in range(1, ntp):
        sums = sums + stat[j]
    d = float(dw * ntp)
    padded = jnp.concatenate([sums, jnp.zeros((120, tb), F32)], axis=0)
    for n in range(tb // 128):
        rows = slice(n * 128, (n + 1) * 128)
        both = padded[:, rows].T
        center = both[:, 0:1] / d
        spread = both[:, 1:2] / d - center * center
        out_ref[rows, :] = (
            (mine[rows, :] - center) * lax.rsqrt(spread + EPSILON) * gain_ref[:, at] + shift_ref[:, at]
        ).astype(BF16)

    for n in range(nx):
        smail.sent(n, sbuf.at[n], sibling)
    for n in range(nx - 1):
        xmail.sent(n, xbuf.at[n], sibling)
    for r in range(1, ntp):
        tmail.sent(r, stat.at[me], sibling)


def down_project(nx, act, dw, fo, gain, shift):
    tb = act.shape[0]
    width = fo.shape[1]
    ntp = 2 * nx
    w = width // ntp
    vm = pl.BlockSpec(memory_space=pltpu.VMEM)
    dma = pltpu.SemaphoreType.DMA
    return pl.pallas_call(
        functools.partial(down_kernel, nx),
        out_shape=jax.ShapeDtypeStruct((tb, w), BF16),
        in_specs=[vm] * 5,
        out_specs=vm,
        scratch_shapes=[
            pltpu.VMEM((nx, tb, w), BF16),
            pltpu.VMEM((nx, tb, w), BF16),
            pltpu.VMEM((nx - 1, tb, w), BF16),
            pltpu.VMEM((nx - 1, tb, w), BF16),
            pltpu.VMEM((tb, w), F32),
            pltpu.VMEM((tb, 128), F32),
            pltpu.VMEM((ntp, 8, tb), F32),
            dma((nx,)),
            dma((nx,)),
            dma((nx,)),
            dma((nx,)),
            dma((ntp,)),
            dma((ntp,)),
        ],
        compiler_params=pltpu.CompilerParams(
            collective_id=1, has_side_effects=True, vmem_limit_bytes=32 * 1024 * 1024
        ),
        cost_estimate=pl.CostEstimate(flops=4_000_000_000, bytes_accessed=8_000_000, transcendentals=0),
        name="down_project",
    )(act, dw, fo, gain, shift)


def body(nz, ny, nx, queries, keys, values, breaks, residual_in, out_weight, first_gain,
         first_shift, up_weight, down_weight, second_gain, second_shift):
    up_full = lax.all_gather(up_weight, "sp", axis=0, tiled=True)
    down_full = lax.all_gather(down_weight, "sp", axis=0, tiled=True)
    bias = jnp.broadcast_to((breaks.astype(F32) * LOG2E).reshape(1, -1), (8, breaks.shape[0]))
    row = lambda a: a.reshape(1, -1)
    first_out = attention_layer(
        nz, ny, nx, queries, keys, values, bias, out_weight, residual_in,
        row(first_gain), row(first_shift),
    )
    activated = up_project(first_out, up_full)
    return down_project(
        nx, activated, down_full, first_out, row(second_gain), row(second_shift)
    )


def solution(mesh):
    nz, ny = split_sp(mesh.shape["sp"])
    nx = mesh.shape["tp"] // 2
    return jax.shard_map(
        functools.partial(body, nz, ny, nx),
        mesh=mesh,
        in_specs=(
            P("sp", "tp"),
            P("sp", "tp"),
            P("sp", "tp"),
            P("sp", "tp"),
            P("sp", "tp"),
            P("tp", None),
            P(),
            P(),
            P("sp", "tp"),
            P("sp", "tp"),
            P(),
            P(),
        ),
        out_specs=P("sp", "tp"),
        check_vma=False,
    )
```

time: 574 us -> 218 us (0.38)
  the two profiles are of different devices: /device:TPU:120 before, /device:TPU:1 now
where the time goes in v1:
time: 218 us
  Pallas kernels  131 us (60%)
  waiting for transfers between devices  65.5 us (30%)
  between operations  13.4 us (6%)
  local copies, waits for them, and re-layouts  7.28 us (3%)
    pallas_call x1, Pallas kernels, attention_layer(): pl.pallas_call(functools.partial(attention_kernel, nz, ny, nx), out_shape...  98.6 us
    all_gather x1, waiting for transfers between devices, body(): down_full = lax.all_gather(down_weight, 'sp', axis=0, tiled=True)  64.1 us
    pallas_call x1, Pallas kernels, down_project(): pl.pallas_call(functools.partial(down_kernel, nx), out_shape=jax.ShapeDty...  28.4 us
    unnamed x13, local copies, waits for them, and re-layouts  6.67 us
  transfers between devices with their start and end apart: 2, of which 1 were waited for; matrix products, arithmetic and copies ran while one was open for 1% of the time, Pallas kernels for 47%

profile of v1, /device:TPU:1, one launch (start us, length us, event | category | flops | bytes accessed | tf_op | source)
XLA Modules:
  0.0 217.6 jit_solution(10649228187260768606)
XLA Ops:
  6.5 0.0 all-gather.3.cloned.1.call-start
  6.5 0.7 all-gather.3.cloned.1.call-update
  7.3 0.0 all-gather.5.cloned.1.call-start
  7.3 0.7 all-gather.5.cloned.1.call-update
  8.0 0.7 convert_multiply_fusion
  8.7 0.6 broadcast_in_dim.8.b_ref
  9.3 98.6 %attention_layer.1.x_ref.fo_ref = bf16[512,2048]{1,0:T(8,128)(2,1)} custom-call(bf16[512,128]{1,0:T(8,128)(2,1)} %q_ref.1, bf16[512,128]{1,0:T(8,128)(2,1)} %k_ref.1, bf16[512,128]{1,0:T(8,128)(2,1)} %v_ref.1, f32[8,512]{1,0:T(8,128)} %broadcast_in_dim.8.b_ref, bf16[128,2048]{1,0:T(8,128)(2,1)} %ow_ref.1, bf16[512,256]{1,0:T(8,128)(2,1)} %res_ref.1, ...), custom_call_target="tpu_custom_call" | custom-call | flops 20000000000 | bytes 8000000 | tf_op jit(solution)/shard_map/attention_layer/pallas_call | solution.py:381
  107.9 0.0 all-gather.3.cloned.1.call-done.w_ref
  108.0 0.0 copy-start
  108.0 2.2 %copy-done = bf16[2048,1024]{1,0:T(8,128)(2,1)S(1)} copy-done((bf16[2048,1024]{1,0:T(8,128)(2,1)S(1)}, bf16[2048,1024]{1,0:T(8,128)(2,1)}, u32[]{:S(2)}) %copy-start) | copy-done | bytes 4194328
  110.2 0.0 copy-start.4
  110.2 1.6 copy-done.4
  111.7 0.0 copy-start.2
  111.8 0.0 copy-start.3
  111.8 0.0 copy-start.5
  111.8 3.5 %up_project.1.act_ref = bf16[512,1024]{1,0:T(8,128)(2,1)S(1)} custom-call(bf16[512,2048]{1,0:T(8,128)(2,1)S(1)} %copy-done.4, bf16[2048,1024]{1,0:T(8,128)(2,1)S(1)} %copy-done), custom_call_target="tpu_custom_call" | custom-call | flops 2147483648 | bytes 7340032 | tf_op jit(solution)/shard_map/up_project/pallas_call | solution.py:428
  115.3 64.1 %all-gather.5.cloned.1.call-done.dw_ref = bf16[2048,1024]{1,0:T(8,128)(2,1)} async-done(((bf16[64,1024]{1,0:T(8,128)(2,1)}), bf16[2048,1024]{1,0:T(8,128)(2,1)}) %all-gather.5.cloned.1.call-update) | async-done | bytes 4194320 | tf_op jit(solution)/shard_map/all_gather | solution.py:574
  179.4 0.0 copy-done.2
  179.4 0.0 copy-done.3
  179.4 0.0 copy-done.5
  179.4 0.0 copy-start.1
  179.4 2.2 %copy-done.1 = bf16[2048,1024]{1,0:T(8,128)(2,1)S(1)} copy-done((bf16[2048,1024]{1,0:T(8,128)(2,1)S(1)}, bf16[2048,1024]{1,0:T(8,128)(2,1)}, u32[]{:S(2)}) %copy-start.1) | copy-done | bytes 4194328
  181.6 28.4 %down_project.1 = bf16[512,256]{1,0:T(8,128)(2,1)S(1)} custom-call(bf16[512,1024]{1,0:T(8,128)(2,1)S(1)} %up_project.1.act_ref, bf16[2048,1024]{1,0:T(8,128)(2,1)S(1)} %copy-done.1, bf16[512,2048]{1,0:T(8,128)(2,1)S(1)} %copy-done.5, f32[1,2048]{1,0:T(1,128)S(1)} %bitcast.5, f32[1,2048]{1,0:T(1,128)S(1)} %bitcast.6), custom_call_target="tpu_custom_call" | custom-call | flops 4000000000 | bytes 8000000 | tf_op jit(solution)/shard_map/down_project/pallas_call | solution.py:543
  210.1 0.7 copy.14
Async XLA Ops:
  6.5 101.4 %all-gather.3.cloned.1.call-start = ((), (), s32[]{:S(2)}) async-start(), calls=%async_computation | async-start | bytes 4325376 | tf_op jit(solution)/shard_map/all_gather | solution.py:573
  7.3 172.1 %all-gather.5.cloned.1.call-start = ((), (), s32[]{:S(2)}) async-start(), calls=%async_computation.1 | async-start | bytes 4325376 | tf_op jit(solution)/shard_map/all_gather | solution.py:574
  108.0 2.2 %copy-start = (bf16[2048,1024]{1,0:T(8,128)(2,1)S(1)}, bf16[2048,1024]{1,0:T(8,128)(2,1)}, u32[]{:S(2)}) copy-start(bf16[2048,1024]{1,0:T(8,128)(2,1)} %all-gather.3.cloned.1.call-done.w_ref) | copy-start | bytes 12582916
  110.2 1.6 copy-start.4
  111.7 67.7 %copy-start.2 = (f32[2048]{0:T(1024)S(1)}, f32[2048]{0:T(1024)}, u32[]{:S(2)}) copy-start(f32[2048]{0:T(1024)} %param.22) | copy-start | bytes 24580
  111.8 67.7 %copy-start.3 = (f32[2048]{0:T(1024)S(1)}, f32[2048]{0:T(1024)}, u32[]{:S(2)}) copy-start(f32[2048]{0:T(1024)} %param.23) | copy-start | bytes 24580
  111.8 67.7 %copy-start.5 = (bf16[512,2048]{1,0:T(8,128)(2,1)S(1)}, bf16[512,2048]{1,0:T(8,128)(2,1)}, u32[]{:S(2)}) copy-start(bf16[512,2048]{1,0:T(8,128)(2,1)} %attention_layer.1.x_ref.fo_ref) | copy-start | bytes 6291460
  179.4 2.2 %copy-start.1 = (bf16[2048,1024]{1,0:T(8,128)(2,1)S(1)}, bf16[2048,1024]{1,0:T(8,128)(2,1)}, u32[]{:S(2)}) copy-start(bf16[2048,1024]{1,0:T(8,128)(2,1)} %all-gather.5.cloned.1.call-done.dw_ref) | copy-start | bytes 12582916
Sparse Core Ops, SparseCore 0:
  9.9 87.9 all-gather.2
  100.4 78.9 all-gather.4

commit v2 on v1

--- a/solution.py
+++ b/solution.py
@@ -19,7 +19,7 @@
 
 
 def split_sp(n_sp):
-    ny = 4 if n_sp == 32 else 2
+    ny = 4 if n_sp >= 16 else 2
     return n_sp // ny, ny
 
 
@@ -31,18 +31,18 @@
     def __init__(self, send, recv):
         self.send, self.recv = send, recv
 
-    def make(self, m, src, dst, target):
+    def make(self, m, src, dst, target, there=None):
         return pltpu.make_async_remote_copy(
             src_ref=src,
             dst_ref=dst,
             send_sem=self.send.at[m],
-            recv_sem=self.recv.at[m],
+            recv_sem=self.recv.at[m if there is None else there],
             device_id=target,
             device_id_type=MESH,
         )
 
-    def start(self, m, src, dst, target):
-        self.make(m, src, dst, target).start()
+    def start(self, m, src, dst, target, there=None):
+        self.make(m, src, dst, target, there).start()
 
     def arrived(self, m, dst, target):
         self.make(m, dst, dst, target).wait_recv()
@@ -89,13 +89,17 @@
             self.mail.sent(self.base + self.nx + r, self.slot(self.me), self.sib)
 
 
-def attention_kernel(
+def layer_kernel(
     nz, ny, nx,
     q_ref, k_ref, v_ref, b_ref, ow_ref, res_ref, gain_ref, shift_ref,
-    fo_ref,
+    uw_ref, dw_ref, gain2_ref, shift2_ref,
+    out_ref,
     qbuf, kb, vb, bb, tri, pacc, tcol, tt, fac, part, partf, prec, stage,
-    ow_full, res_full, att_full, pre,
+    ow_full, res_full, att_full, pre, fo_ref,
+    up_full, down_full, act, hold, sbuf, sib, xbuf, rbuf, mine, cols, stat,
     msend, mrecv, ksend, krecv, vsend, vrecv,
+    usend, urecv, ysend, yrecv, dsend, drecv,
+    ssend, srecv, xsend, xrecv, tsend, trecv,
 ):
     sp = lax.axis_index("sp")
     z, y = sp // ny, lax.rem(sp, ny)
@@ -105,6 +109,8 @@
     rows = 2 * ny * half
     mail = Mail(msend, mrecv)
     kmail, vmail = Mail(ksend, krecv), Mail(vsend, vrecv)
+    umail, ymail, dmail = Mail(usend, urecv), Mail(ysend, yrecv), Mail(dsend, drecv)
+    wr = uw_ref.shape[0]
 
     def zdev(zz):
         return {"sp": zz * ny + y}
@@ -113,6 +119,24 @@
         return {"sp": z * ny + lax.rem(y + ny + r, ny)}
 
     mirror = zdev(nz - 1 - z)
+
+    def zof(i):
+        odd, step = lax.rem(i, 2), (i + 1) // 2
+        return lax.rem(jnp.where(odd == 1, z - step, z + step) + nz, nz)
+
+    def up_slab(zz, r, part=None):
+        at = (zz * ny + lax.rem(y + ny + r, ny)) * wr
+        n = wr if part is None else wr // 2
+        return up_full.at[pl.ds(pl.multiple_of(at + (part or 0) * n, n), n), :]
+
+    dh = ny * wr // 2
+
+    def down_half(zz, h):
+        return down_full.at[pl.ds(pl.multiple_of((zz * 2 + h) * dh, dh), dh), :]
+
+    def down_slab(r):
+        at = (z * ny + lax.rem(y + ny + r, ny)) * wr
+        return down_full.at[pl.ds(pl.multiple_of(at, wr), wr), :]
 
     barrier = pltpu.get_barrier_semaphore()
     for r in range(1, nz):
@@ -130,7 +154,8 @@
     m_t = m_b + nz
     m_p = m_t + ny
     m_ret = m_p + ny
-    g0 = m_ret + 1
+    m_d = m_ret + 1
+    g0 = m_d + ny
     gn = Gather.count(nx)
     g_ow = Gather(mail, g0, lambda j: ow_full.at[pl.ds(j * hd, hd), :], nx)
     dw = res_ref.shape[1]
@@ -160,8 +185,38 @@
     kmail.start(2, k_ref, kb.at[2], left)
     vmail.start(1, v_ref, vb.at[1], right)
     vmail.start(2, v_ref, vb.at[2], left)
+    umail.start(1, uw_ref, up_slab(z, 0), right)
+    umail.start(2, uw_ref, up_slab(z, 0), left)
+    for r in range(1, ny):
+        mail.start(m_d + r, dw_ref, down_slab(0), ydev(r))
+
+    def pass_up(i, src):
+        slab = up_slab(zof(i), 0)
+        ymail.start(4 * i, slab if src is None else src, slab, ydev(1))
+        if ny > 2:
+            ymail.start(4 * i + 1, slab if src is None else src, slab, ydev(-1))
+
+    def relay_up(i):
+        if ny > 2:
+            zz = zof(i)
+            ymail.arrived(4 * i, up_slab(zz, -1), ydev(-1))
+            ymail.start(4 * i + 2, up_slab(zz, -1, 0), up_slab(zz, -1, 0), ydev(1))
+            ymail.arrived(4 * i + 1, up_slab(zz, 1), ydev(1))
+            ymail.start(4 * i + 3, up_slab(zz, 1, 1), up_slab(zz, 1, 1), ydev(-1))
+
+    def take_up(i):
+        zz = zof(i)
+        if ny > 2:
+            ymail.arrived(4 * i + 2, up_slab(zz, -2, 0), ydev(-1))
+            ymail.arrived(4 * i + 3, up_slab(zz, 2, 1), ydev(1))
+        else:
+            ymail.arrived(4 * i, up_slab(zz, -1), ydev(-1))
+
+    pass_up(0, uw_ref)
     g_ow.start(ow_ref)
     g_res.start(res_ref)
+    up_slab(z, 0)[...] = uw_ref[...]
+    down_slab(0)[...] = dw_ref[...]
 
     qbuf[y] = q_ref[:half, :]
     bb[z] = b_ref[...]
@@ -190,8 +245,7 @@
     @pl.loop(0, nz)
     def _(i):
         odd = lax.rem(i, 2)
-        step = (i + 1) // 2
-        zb = lax.rem(jnp.where(odd == 1, z - step, z + step) + nz, nz)
+        zb = zof(i)
         onward = zdev(lax.rem(jnp.where(odd == 1, z + 1, z - 1) + nz, nz))
 
         @pl.when(i > 0)
@@ -257,6 +311,45 @@
                 where = pl.ds(pl.multiple_of(t * half, half), half)
                 pacc[zb, where, :] = jnp.zeros((half, hd), F32)
 
+        @pl.when(jnp.logical_and(i > 0, i < nz - 1))
+        def _():
+            umail.arrived(i, up_slab(zb, 0), onward)
+
+        @pl.when(jnp.logical_and(i >= 1, i <= nz - 4))
+        def _():
+            umail.start(i + 2, up_slab(zb, 0), up_slab(zb, 0), onward)
+
+        @pl.when(i == nz - 3)
+        def _():
+            umail.start(nz - 1, up_slab(zb, 0, 0), up_slab(zb, 0, 0), onward)
+
+        @pl.when(i == nz - 2)
+        def _():
+            umail.start(nz, up_slab(zb, 0, 1), up_slab(zb, 0, 1), onward)
+            for r in range(1, ny):
+                mail.arrived(m_d + r, down_slab(-r), ydev(r))
+            for h in range(2):
+                for j, to in ((1, right), (2, left)):
+                    dmail.start(2 * j + h, down_half(z, h), down_half(z, h), to)
+
+        @pl.when(jnp.logical_and(i > 0, i < nz - 1))
+        def _():
+            pass_up(i, None)
+
+        @pl.when(i >= 2)
+        def _():
+            relay_up(i - 2)
+
+    def down_step(step):
+        for h in range(2):
+            for i, to in ((2 * step - 1, right), (2 * step, left)):
+                zz = zof(i)
+                dmail.arrived(2 * i + h, down_half(zz, h), to)
+                if i + 2 < nz - 1:
+                    dmail.start(2 * (i + 2) + h, down_half(zz, h), down_half(zz, h), to)
+                elif (i + h) % 2 == 1:
+                    dmail.start(2 * (nz - 1) + h, down_half(zz, h), down_half(zz, h), to)
+
     @pl.loop(0, rows // 128)
     def _(n):
         at = pl.ds(pl.multiple_of(n * 128, 128), 128)
@@ -264,6 +357,10 @@
 
     for r in range(1, ny):
         mail.start(m_t + r, tt.at[y], tt.at[y], ydev(r))
+    last = zof(nz - 1)
+    umail.arrived(nz - 1, up_slab(last, 0, 0), left)
+    umail.arrived(nz, up_slab(last, 0, 1), right)
+    pass_up(nz - 1, None)
     g_ow.forward()
     g_res.forward()
     for r in range(1, ny):
@@ -297,6 +394,7 @@
             to = lax.rem(y + r, ny)
             src = part.at[pl.ds(pl.multiple_of((h * ny + to) * half, half), half), :]
             mail.start(m_p + r if h == 0 else m_p2(m_p, r, g0, gn), src, prec.at[y, h], ydev(r))
+    relay_up(nz - 2)
     own = lambda h: partf[pl.ds(pl.multiple_of((h * ny + y) * half, half), half), :]
 
     def summed(h):
@@ -310,8 +408,11 @@
     mycol = pl.ds(pl.multiple_of(me * hd, hd), hd)
     stage[...] = summed(1)
     mail.start(m_ret, stage, att_full.at[pl.ds(half, half), mycol], mirror)
+    relay_up(nz - 1)
     att_full[:half, mycol] = summed(0)
     g_att[0].start(att_full.at[pl.ds(0, half), mycol])
+    if nz > 4:
+        down_step(1)
     mail.arrived(m_ret, att_full.at[pl.ds(half, half), mycol], mirror)
     g_att[1].start(att_full.at[pl.ds(half, half), mycol])
     g_ow.finish()
@@ -331,6 +432,8 @@
             ALPHA * res_full[:, at].astype(F32)
         )
 
+    if nz > 6:
+        down_step(2)
     rc = 64
 
     @pl.loop(0, tb // rc)
@@ -344,6 +447,109 @@
             BF16
         )
 
+    for i in range(nz):
+        take_up(i)
+    hidden = up_full.shape[1]
+    hc = min(256, hidden)
+
+    @pl.loop(0, hidden // hc)
+    def _(n):
+        at = pl.ds(pl.multiple_of(n * hc, hc), hc)
+        h = jnp.maximum(jnp.dot(fo_ref[...], up_full[:, at], preferred_element_type=F32), 0.0)
+        act[:, at] = (h * h).astype(BF16)
+
+    ntp = 2 * nx
+    x, c = me // 2, lax.rem(me, 2)
+    smail, xmail, tmail = Mail(ssend, srecv), Mail(xsend, xrecv), Mail(tsend, trecv)
+    sibling = {"tp": x * 2 + 1 - c}
+    fw = out_ref.shape[1]
+
+    def mix(i):
+        j = zof(i)
+        chip = j // 2
+        piece = lax.dot_general(
+            act[...],
+            down_full[pl.ds(pl.multiple_of(j * fw, fw), fw), :],
+            NT,
+            preferred_element_type=F32,
+        )
+
+        @pl.when(lax.rem(j, 2) != c)
+        def _():
+            sbuf[chip] = piece.astype(BF16)
+            smail.start(chip, sbuf.at[chip], sib.at[chip], sibling)
+
+        @pl.when(lax.rem(j, 2) == c)
+        def _():
+            hold[...] = piece
+
+    def settle(i):
+        j = zof(i)
+        chip = j // 2
+
+        @pl.when(lax.rem(j, 2) == c)
+        def _():
+            smail.arrived(chip, sib.at[chip], sibling)
+            both = hold[...] + sib[chip].astype(F32)
+
+            @pl.when(chip != x)
+            def _():
+                xbuf[chip] = both.astype(BF16)
+                xmail.start(chip, xbuf.at[chip], rbuf.at[x], {"tp": j}, there=x)
+
+            @pl.when(chip == x)
+            def _():
+                mine[...] = both
+
+    final = nz // 2 - 1
+
+    @pl.loop(0, nz)
+    def _(i):
+        @pl.when(i == nz - 3)
+        def _():
+            down_step(final)
+
+        @pl.when(i == nz - 1)
+        def _():
+            zz = zof(nz - 1)
+            dmail.arrived(2 * (nz - 1), down_half(zz, 0), left)
+            dmail.arrived(2 * (nz - 1) + 1, down_half(zz, 1), right)
+
+        mix(i)
+        settle(i)
+
+    at = pl.ds(pl.multiple_of(me * fw, fw), fw)
+    mine[...] = mine[...] + ALPHA * fo_ref[:, at].astype(F32)
+    for r in range(1, nx):
+        n = lax.rem(x + r, nx)
+        xmail.arrived(n, rbuf.at[n], sibling)
+        mine[...] = mine[...] + rbuf[n].astype(F32)
+    total = mine[...]
+    row_sum = jnp.sum(total, axis=-1, keepdims=True)
+    row_squares = jnp.sum(total * total, axis=-1, keepdims=True)
+    lane = iota((tb, 128), 1)
+    cols[...] = jnp.where(lane == 0, row_sum, jnp.where(lane == 1, row_squares, 0.0))
+    for n in range(tb // 128):
+        stat[me, :, n * 128 : (n + 1) * 128] = cols[n * 128 : (n + 1) * 128, :].T[:8, :]
+    for r in range(1, ntp):
+        tmail.start(r, stat.at[me], stat.at[me], {"tp": lax.rem(me + r, ntp)})
+    for r in range(1, ntp):
+        tmail.arrived(r, stat.at[lax.rem(me + ntp - r, ntp)], sibling)
+    sums = stat[0]
+    for j in range(1, ntp):
+        sums = sums + stat[j]
+    d = float(fw * ntp)
+    padded = jnp.concatenate([sums, jnp.zeros((120, tb), F32)], axis=0)
+    for n in range(tb // 128):
+        rows_n = slice(n * 128, (n + 1) * 128)
+        both = padded[:, rows_n].T
+        center = both[:, 0:1] / d
+        spread = both[:, 1:2] / d - center * center
+        out_ref[rows_n, :] = (
+            (mine[rows_n, :] - center) * lax.rsqrt(spread + EPSILON) * gain2_ref[:, at]
+            + shift2_ref[:, at]
+        ).astype(BF16)
+
     mail.sent(m_q2, late, mirror)
     for r in range(1, ny):
         mail.sent(m_q1 + r, early, mirror)
@@ -354,6 +560,25 @@
     for r in range(1, nz):
         mail.sent(m_b + r, b_ref, mirror)
     mail.sent(m_ret, stage, mirror)
+    for r in range(1, ny):
+        mail.sent(m_d + r, dw_ref, mirror)
+    for i in range(1, nz + 1):
+        umail.sent(i, up_slab(0, 0) if i < nz - 1 else up_slab(0, 0, 0), mirror)
+    for i in range(nz):
+        ymail.sent(4 * i, up_slab(0, 0), mirror)
+        if ny > 2:
+            ymail.sent(4 * i + 1, up_slab(0, 0), mirror)
+            ymail.sent(4 * i + 2, up_slab(0, 0, 0), mirror)
+            ymail.sent(4 * i + 3, up_slab(0, 0, 0), mirror)
+    for i in range(1, nz):
+        for h in range(2):
+            dmail.sent(2 * i + h, down_half(0, 0), mirror)
+    for n in range(nx):
+        smail.sent(n, sbuf.at[0], sibling)
+    for r in range(1, nx):
+        xmail.sent(lax.rem(x + r, nx), rbuf.at[0], sibling)
+    for r in range(1, ntp):
+        tmail.sent(r, stat.at[me], sibling)
 
     @pl.loop(1, nz)
     def _(i):
@@ -368,20 +593,22 @@
     return g0 + 4 * gn + r
 
 
-def attention_layer(nz, ny, nx, q, k, v, bias, ow, res, gain, shift):
+def layer(nz, ny, nx, q, k, v, bias, ow, res, gain, shift, uw, dw, gain2, shift2):
     tb, hd = q.shape
     half = tb // 2
     rows = 2 * ny * half
     width = ow.shape[1]
     ntp = 2 * nx
-    gn = Gather.count(nx)
-    messages = 3 * ny + nz + 2 * ny + 1 + 4 * gn + ny
+    fw = width // ntp
+    hidden = uw.shape[1]
+    messages = 3 * ny + nz + 2 * ny + 1 + ny + 4 * Gather.count(nx) + ny
     vm = pl.BlockSpec(memory_space=pltpu.VMEM)
     dma = pltpu.SemaphoreType.DMA
+    pairs = [messages, nz, nz, nz + 1, 4 * nz, 2 * nz, nx, nx, ntp]
     return pl.pallas_call(
-        functools.partial(attention_kernel, nz, ny, nx),
-        out_shape=jax.ShapeDtypeStruct((tb, width), BF16),
-        in_specs=[vm] * 8,
+        functools.partial(layer_kernel, nz, ny, nx),
+        out_shape=jax.ShapeDtypeStruct((tb, fw), BF16),
+        in_specs=[vm] * 12,
         out_specs=vm,
         scratch_shapes=[
             pltpu.VMEM((2 * ny, half, hd), BF16),
@@ -401,186 +628,34 @@
             pltpu.VMEM((tb, width), BF16),
             pltpu.VMEM((tb, ntp * hd), BF16),
             pltpu.VMEM((tb, width), F32),
-            dma((messages,)),
-            dma((messages,)),
-            dma((nz,)),
-            dma((nz,)),
-            dma((nz,)),
-            dma((nz,)),
-        ],
-        compiler_params=pltpu.CompilerParams(
-            collective_id=0, has_side_effects=True, vmem_limit_bytes=56 * 1024 * 1024
-        ),
-        cost_estimate=pl.CostEstimate(flops=20_000_000_000, bytes_accessed=8_000_000, transcendentals=0),
-        name="attention_layer",
-    )(q, k, v, bias, ow, res, gain, shift)
-
-
-def up_kernel(x_ref, w_ref, o_ref):
-    hidden = jnp.maximum(jnp.dot(x_ref[...], w_ref[...], preferred_element_type=F32), 0.0)
-    o_ref[...] = (hidden * hidden).astype(BF16)
-
-
-def up_project(x, w):
-    tb, d = x.shape
-    n = w.shape[1]
-    nb = min(256, n)
-    return pl.pallas_call(
-        up_kernel,
-        out_shape=jax.ShapeDtypeStruct((tb, n), BF16),
-        grid=(n // nb,),
-        in_specs=[
-            pl.BlockSpec((tb, d), lambda i: (0, 0)),
-            pl.BlockSpec((d, nb), lambda i: (0, i)),
-        ],
-        out_specs=pl.BlockSpec((tb, nb), lambda i: (0, i)),
-        compiler_params=pltpu.CompilerParams(vmem_limit_bytes=24 * 1024 * 1024),
-        cost_estimate=pl.CostEstimate(
-            flops=2 * tb * d * n, bytes_accessed=2 * (tb * d + d * n + tb * n), transcendentals=0
-        ),
-        name="up_project",
-    )(x, w)
-
-
-def down_kernel(
-    nx,
-    act_ref, dw_ref, fo_ref, gain_ref, shift_ref,
-    out_ref,
-    sbuf, sib, xbuf, rbuf, mine, cols, stat,
-    ssend, srecv, xsend, xrecv, tsend, trecv,
-):
-    me = lax.axis_index("tp")
-    x, c = me // 2, lax.rem(me, 2)
-    ntp = 2 * nx
-    tb, dw = out_ref.shape
-    smail, xmail, tmail = Mail(ssend, srecv), Mail(xsend, xrecv), Mail(tsend, trecv)
-    sibling = {"tp": x * 2 + 1 - c}
-
-    barrier = pltpu.get_barrier_semaphore()
-    for r in range(1, ntp):
-        pl.semaphore_signal(
-            barrier, inc=1, device_id={"tp": lax.rem(me + r, ntp)}, device_id_type=MESH
-        )
-    pl.semaphore_wait(barrier, ntp - 1)
-
-    @pl.loop(0, ntp)
-    def _(i):
-        first = i < nx
-        n = lax.rem(i, nx)
-        chip = lax.rem(x + 1 + n, nx)
-        j = chip * 2 + jnp.where(first, 1 - c, c)
-        piece = lax.dot_general(
-            act_ref[...],
-            dw_ref[pl.ds(pl.multiple_of(j * dw, dw), dw), :],
-            NT,
-            preferred_element_type=F32,
-        )
-
-        @pl.when(first)
-        def _():
-            sbuf[n] = piece.astype(BF16)
-            smail.start(n, sbuf.at[n], sib.at[n], sibling)
-
-        @pl.when(jnp.logical_not(first))
-        def _():
-            smail.arrived(n, sib.at[n], sibling)
-            both = piece + sib[n].astype(F32)
-
-            @pl.when(n < nx - 1)
-            def _():
-                xbuf[n] = both.astype(BF16)
-                xmail.start(n, xbuf.at[n], rbuf.at[n], {"tp": j})
-
-            @pl.when(n == nx - 1)
-            def _():
-                mine[...] = both
-
-    at = pl.ds(pl.multiple_of(me * dw, dw), dw)
-    total = mine[...] + ALPHA * fo_ref[:, at].astype(F32)
-    for n in range(nx - 1):
-        xmail.arrived(n, rbuf.at[n], sibling)
-        total = total + rbuf[n].astype(F32)
-    mine[...] = total
-    row_sum = jnp.sum(total, axis=-1, keepdims=True)
-    row_squares = jnp.sum(total * total, axis=-1, keepdims=True)
-    lane = iota((tb, 128), 1)
-    cols[...] = jnp.where(lane == 0, row_sum, jnp.where(lane == 1, row_squares, 0.0))
-    for n in range(tb // 128):
-        stat[me, :, n * 128 : (n + 1) * 128] = cols[n * 128 : (n + 1) * 128, :].T[:8, :]
-    for r in range(1, ntp):
-        tmail.start(r, stat.at[me], stat.at[me], {"tp": lax.rem(me + r, ntp)})
-    for r in range(1, ntp):
-        tmail.arrived(r, stat.at[lax.rem(me + ntp - r, ntp)], sibling)
-    sums = stat[0]
-    for j in range(1, ntp):
-        sums = sums + stat[j]
-    d = float(dw * ntp)
-    padded = jnp.concatenate([sums, jnp.zeros((120, tb), F32)], axis=0)
-    for n in range(tb // 128):
-        rows = slice(n * 128, (n + 1) * 128)
-        both = padded[:, rows].T
-        center = both[:, 0:1] / d
-        spread = both[:, 1:2] / d - center * center
-        out_ref[rows, :] = (
-            (mine[rows, :] - center) * lax.rsqrt(spread + EPSILON) * gain_ref[:, at] + shift_ref[:, at]
-        ).astype(BF16)
-
-    for n in range(nx):
-        smail.sent(n, sbuf.at[n], sibling)
-    for n in range(nx - 1):
-        xmail.sent(n, xbuf.at[n], sibling)
-    for r in range(1, ntp):
-        tmail.sent(r, stat.at[me], sibling)
-
-
-def down_project(nx, act, dw, fo, gain, shift):
-    tb = act.shape[0]
-    width = fo.shape[1]
-    ntp = 2 * nx
-    w = width // ntp
-    vm = pl.BlockSpec(memory_space=pltpu.VMEM)
-    dma = pltpu.SemaphoreType.DMA
-    return pl.pallas_call(
-        functools.partial(down_kernel, nx),
-        out_shape=jax.ShapeDtypeStruct((tb, w), BF16),
-        in_specs=[vm] * 5,
-        out_specs=vm,
-        scratch_shapes=[
-            pltpu.VMEM((nx, tb, w), BF16),
-            pltpu.VMEM((nx, tb, w), BF16),
-            pltpu.VMEM((nx - 1, tb, w), BF16),
-            pltpu.VMEM((nx - 1, tb, w), BF16),
-            pltpu.VMEM((tb, w), F32),
+            pltpu.VMEM((tb, width), BF16),
+            pltpu.VMEM((width, hidden), BF16),
+            pltpu.VMEM((width, hidden), BF16),
+            pltpu.VMEM((tb, hidden), BF16),
+            pltpu.VMEM((tb, fw), F32),
+            pltpu.VMEM((nx, tb, fw), BF16),
+            pltpu.VMEM((nx, tb, fw), BF16),
+            pltpu.VMEM((nx, tb, fw), BF16),
+            pltpu.VMEM((nx, tb, fw), BF16),
+            pltpu.VMEM((tb, fw), F32),
             pltpu.VMEM((tb, 128), F32),
             pltpu.VMEM((ntp, 8, tb), F32),
-            dma((nx,)),
-            dma((nx,)),
-            dma((nx,)),
-            dma((nx,)),
-            dma((ntp,)),
-            dma((ntp,)),
-        ],
+        ]
+        + [dma((n,)) for n in pairs for _ in range(2)],
         compiler_params=pltpu.CompilerParams(
-            collective_id=1, has_side_effects=True, vmem_limit_bytes=32 * 1024 * 1024
+            collective_id=0, has_side_effects=True, vmem_limit_bytes=60 * 1024 * 1024
         ),
-        cost_estimate=pl.CostEstimate(flops=4_000_000_000, bytes_accessed=8_000_000, transcendentals=0),
-        name="down_project",
-    )(act, dw, fo, gain, shift)
+        name="layer",
+    )(q, k, v, bias, ow, res, gain, shift, uw, dw, gain2, shift2)
 
 
 def body(nz, ny, nx, queries, keys, values, breaks, residual_in, out_weight, first_gain,
          first_shift, up_weight, down_weight, second_gain, second_shift):
-    up_full = lax.all_gather(up_weight, "sp", axis=0, tiled=True)
-    down_full = lax.all_gather(down_weight, "sp", axis=0, tiled=True)
     bias = jnp.broadcast_to((breaks.astype(F32) * LOG2E).reshape(1, -1), (8, breaks.shape[0]))
     row = lambda a: a.reshape(1, -1)
-    first_out = attention_layer(
+    return layer(
         nz, ny, nx, queries, keys, values, bias, out_weight, residual_in,
-        row(first_gain), row(first_shift),
-    )
-    activated = up_project(first_out, up_full)
-    return down_project(
-        nx, activated, down_full, first_out, row(second_gain), row(second_shift)
+        row(first_gain), row(first_shift), up_weight, down_weight, row(second_gain), row(second_shift),
     )
 
 

time: 218 us -> 138 us (0.63)
  waiting for transfers between devices: 65.5 us -> 0 us
  between operations: 13.4 us -> 0.01 us
  local copies, waits for them, and re-layouts: 7.28 us -> 2.96 us
  Pallas kernels: 131 us -> 135 us
    all_gather x2 -> x0, waiting for transfers between devices: 64.1 us -> none  [the longest x1 64.1 us: body(): down_full = lax.all_gather(down_weight, 'sp', axis=0, tiled=True)]
    unnamed x13 -> x3, local copies, waits for them, and re-layouts: 6.67 us -> 2.35 us
    pallas_call x3 -> x1, Pallas kernels: 131 us -> 135 us  [layer(): pl.pallas_call(functools.partial(layer_kernel, nz, ny, nx), out_shape=jax...]
  transfers between devices with their start and end apart: 2 -> 0, of which waited for: 1 -> 0; matrix products, arithmetic and copies ran while one was open for 1% -> 0% of each run, Pallas kernels for 47% -> 0%
where the time goes in v2:
time: 138 us
  Pallas kernels  135 us (98%)
  local copies, waits for them, and re-layouts  2.96 us (2%)
    pallas_call x1, Pallas kernels, layer(): pl.pallas_call(functools.partial(layer_kernel, nz, ny, nx), out_shape=jax...  135 us

profile of v2, /device:TPU:1, one launch (start us, length us, event | category | flops | bytes accessed | tf_op | source)
XLA Modules:
  0.0 137.5 jit_solution(5771917683529804915)
XLA Ops:
  0.0 0.0 copy-start
  0.0 0.7 copy-done
  0.7 0.6 broadcast_in_dim.8.b_ref
  1.3 134.5 %layer.1 = bf16[512,256]{1,0:T(8,128)(2,1)} custom-call(bf16[512,128]{1,0:T(8,128)(2,1)} %q_ref.1, bf16[512,128]{1,0:T(8,128)(2,1)} %k_ref.1, bf16[512,128]{1,0:T(8,128)(2,1)} %v_ref.1, f32[8,512]{1,0:T(8,128)} %broadcast_in_dim.8.b_ref, bf16[128,2048]{1,0:T(8,128)(2,1)} %ow_ref.1, bf16[512,256]{1,0:T(8,128)(2,1)} %res_ref.1, f32[1,2048]{1,0:T(1,128)} %bitcast.5, ...), custom_call_target="tpu_custom_call" | custom-call | tf_op jit(solution)/shard_map/layer/pallas_call | solution.py:608
  135.8 1.7 %copy.14 = bf16[512,256]{1,0:T(8,128)(2,1)} copy(bf16[512,256]{1,0:T(8,128)(2,1)} %layer.1) | data formatting | bytes 524288
  (1 shorter events, 0.0 us)
Async XLA Ops:
  0.0 0.7 copy-start

commit v3 on v2

--- a/solution.py
+++ b/solution.py
@@ -94,7 +94,7 @@
     q_ref, k_ref, v_ref, b_ref, ow_ref, res_ref, gain_ref, shift_ref,
     uw_ref, dw_ref, gain2_ref, shift2_ref,
     out_ref,
-    qbuf, kb, vb, bb, tri, pacc, tcol, tt, fac, part, partf, prec, stage,
+    qbuf, kb, vb, bb, tri, pacc, tt, fac, part, partf, prec,
     ow_full, res_full, att_full, pre, fo_ref,
     up_full, down_full, act, hold, sbuf, sib, xbuf, rbuf, mine, cols, stat,
     msend, mrecv, ksend, krecv, vsend, vrecv,
@@ -106,7 +106,7 @@
     me = lax.axis_index("tp")
     tb, hd = k_ref.shape
     half = tb // 2
-    rows = 2 * ny * half
+    rows = ny * tb
     mail = Mail(msend, mrecv)
     kmail, vmail = Mail(ksend, krecv), Mail(vsend, vrecv)
     umail, ymail, dmail = Mail(usend, urecv), Mail(ysend, yrecv), Mail(dsend, drecv)
@@ -117,8 +117,6 @@
 
     def ydev(r):
         return {"sp": z * ny + lax.rem(y + ny + r, ny)}
-
-    mirror = zdev(nz - 1 - z)
 
     def zof(i):
         odd, step = lax.rem(i, 2), (i + 1) // 2
@@ -149,12 +147,11 @@
         )
     pl.semaphore_wait(barrier, nz - 1 + ny - 1 + 2 * nx - 1)
 
-    m_q1, m_q2, m_q2f = 0, ny, 2 * ny
-    m_b = 3 * ny
+    m_q = 0
+    m_b = ny
     m_t = m_b + nz
     m_p = m_t + ny
-    m_ret = m_p + ny
-    m_d = m_ret + 1
+    m_d = m_p + ny
     g0 = m_d + ny
     gn = Gather.count(nx)
     g_ow = Gather(mail, g0, lambda j: ow_full.at[pl.ds(j * hd, hd), :], nx)
@@ -174,17 +171,17 @@
         for h in range(2)
     ]
 
-    early, late = q_ref.at[pl.ds(0, half), :], q_ref.at[pl.ds(half, half), :]
-    mail.start(m_q2, late, qbuf.at[ny + y], mirror)
-    for r in range(1, ny):
-        mail.start(m_q1 + r, early, qbuf.at[y], ydev(r))
-    for r in range(1, nz):
-        mail.start(m_b + r, b_ref, bb.at[z], zdev(lax.rem(z + r, nz)))
     right, left = zdev(lax.rem(z + 1, nz)), zdev(lax.rem(z + nz - 1, nz))
     kmail.start(1, k_ref, kb.at[1], right)
     kmail.start(2, k_ref, kb.at[2], left)
-    vmail.start(1, v_ref, vb.at[1], right)
-    vmail.start(2, v_ref, vb.at[2], left)
+    for r in range(1, ny):
+        mail.start(m_q + r, q_ref, qbuf.at[y], ydev(r))
+    vb[0] = v_ref[...].T
+    bb[z] = jnp.broadcast_to(b_ref[...].astype(F32) * LOG2E, (8, tb))
+    vmail.start(1, vb.at[0], vb.at[1], right)
+    vmail.start(2, vb.at[0], vb.at[2], left)
+    for r in range(1, nz):
+        mail.start(m_b + r, bb.at[z], bb.at[z], zdev(lax.rem(z + r, nz)))
     umail.start(1, uw_ref, up_slab(z, 0), right)
     umail.start(2, uw_ref, up_slab(z, 0), left)
     for r in range(1, ny):
@@ -218,29 +215,20 @@
     up_slab(z, 0)[...] = uw_ref[...]
     down_slab(0)[...] = dw_ref[...]
 
-    qbuf[y] = q_ref[:half, :]
-    bb[z] = b_ref[...]
+    qbuf[y] = q_ref[...]
     kb[0] = k_ref[...]
-    vb[0] = v_ref[...]
     ow_full[pl.ds(me * hd, hd), :] = ow_ref[...]
     res_full[:, pl.ds(pl.multiple_of(me * dw, dw), dw)] = res_ref[...]
     tri[...] = (iota((tb, tb), 0) > iota((tb, tb), 1)).astype(BF16)
-    tcol[...] = jnp.zeros_like(tcol)
-    fac[...] = jnp.zeros_like(fac)
-
-    mail.arrived(m_q2, qbuf.at[ny + y], mirror)
-    for r in range(1, ny):
-        mail.start(m_q2f + r, qbuf.at[ny + y], qbuf.at[ny + y], ydev(r))
-    for r in range(1, ny):
-        mail.arrived(m_q1 + r, qbuf.at[lax.rem(y + ny - r, ny)], ydev(r))
-    for r in range(1, ny):
-        mail.arrived(m_q2f + r, qbuf.at[ny + lax.rem(y + ny - r, ny)], ydev(r))
+
+    for r in range(1, ny):
+        mail.arrived(m_q + r, qbuf.at[lax.rem(y + ny - r, ny)], ydev(r))
     for r in range(1, nz):
         mail.arrived(m_b + r, bb.at[lax.rem(z + nz - r, nz)], left)
 
     scale = hd ** (-0.5) * LOG2E
     hk = tb // 2
-    lane = iota((half, 128), 1)
+    ones = jnp.ones((8, tb), BF16)
 
     @pl.loop(0, nz)
     def _(i):
@@ -266,50 +254,63 @@
         def _():
             vmail.start(nz - 1, vb.at[i], vb.at[nz - 1], onward)
 
-        def tile(t, h, masked):
-            where = pl.ds(pl.multiple_of(t * half, half), half)
-            scores = lax.dot_general(qbuf[t], kb[i], NT, preferred_element_type=F32)
-            logits = scores * scale + bb[zb][0:1, :]
-            soft = jnp.maximum(
-                jnp.log(1.0 + jnp.exp2(jnp.minimum(logits, CLAMP))) * LOG2E, logits
-            )
-            brk = logits - soft
-            if masked:
-                strict = iota((half, tb), 1) < iota((half, tb), 0) + h * half
-                soft = jnp.where(strict, soft, 0.0)
-            soft16 = soft.astype(BF16)
-            later0 = jnp.dot(soft16, tri[:, :hk], preferred_element_type=F32)
-            later1 = jnp.dot(soft16[:, hk:], tri[hk:, hk:], preferred_element_type=F32)
-            w0 = jnp.exp2(brk[:, :hk] - later0)
-            w1 = jnp.exp2(brk[:, hk:] - later1)
-            if masked:
-                w0 = jnp.where(strict[:, :hk], w0, 0.0)
-                w1 = jnp.where(strict[:, hk:], w1, 0.0)
-            pacc[zb, where, :] = jnp.dot(
-                w0.astype(BF16), vb[i, :hk, :], preferred_element_type=F32
-            ) + jnp.dot(w1.astype(BF16), vb[i, hk:, :], preferred_element_type=F32)
-            total = later0[:, 0:1] + soft[:, 0:1]
-            tcol[where, :] = jnp.where(lane == zb, total, tcol[where, :])
-
-        @pl.loop(0, 2 * ny)
+        def tile(t, masked):
+            def scored(h):
+                q = qbuf[t, h * half : (h + 1) * half, :]
+                scores = lax.dot_general(q, kb[i], NT, preferred_element_type=F32)
+                logits = scores * scale + bb[zb][0:1, :]
+                soft = jnp.maximum(
+                    jnp.log(1.0 + jnp.exp2(jnp.minimum(logits, CLAMP))) * LOG2E, logits
+                )
+                brk = logits - soft
+                if masked:
+                    soft = jnp.where(strict(h), soft, 0.0)
+                return brk, soft.astype(BF16)
+
+            def strict(h):
+                return iota((half, tb), 1) < iota((half, tb), 0) + h * half
+
+            def weighed(h, brk, soft16):
+                later0 = jnp.dot(soft16, tri[:, :hk], preferred_element_type=F32)
+                later1 = jnp.dot(soft16[:, hk:], tri[hk:, hk:], preferred_element_type=F32)
+                w0 = jnp.exp2(brk[:, :hk] - later0)
+                w1 = jnp.exp2(brk[:, hk:] - later1)
+                if masked:
+                    w0 = jnp.where(strict(h)[:, :hk], w0, 0.0)
+                    w1 = jnp.where(strict(h)[:, hk:], w1, 0.0)
+                return w0.astype(BF16), w1.astype(BF16)
+
+            def finish(h, soft16, w0, w1):
+                where = pl.ds(pl.multiple_of(t * tb + h * half, half), half)
+                pacc[zb, :, where] = lax.dot_general(
+                    vb[i, :, :hk], w0, NT, preferred_element_type=F32
+                ) + lax.dot_general(vb[i, :, hk:], w1, NT, preferred_element_type=F32)
+                total = lax.dot_general(ones, soft16, NT, preferred_element_type=F32)
+                tt[y, pl.ds(zb, 1), where] = total[0:1, :]
+
+            both = [scored(h) for h in range(2)]
+            weights = [weighed(h, *both[h]) for h in range(2)]
+            for h in range(2):
+                finish(h, both[h][1], *weights[h])
+
+        @pl.loop(0, ny)
         def _(t):
-            h = t // ny
-            qz = jnp.where(h == 0, z, nz - 1 - z)
-            qblock = qz * ny + lax.rem(t, ny)
+            qblock = z * ny + t
             kblock = zb * ny + y
 
             @pl.when(kblock < qblock)
             def _():
-                tile(t, h, False)
+                tile(t, False)
 
             @pl.when(kblock == qblock)
             def _():
-                tile(t, h, True)
+                tile(t, True)
 
             @pl.when(kblock > qblock)
             def _():
-                where = pl.ds(pl.multiple_of(t * half, half), half)
-                pacc[zb, where, :] = jnp.zeros((half, hd), F32)
+                where = pl.ds(pl.multiple_of(t * tb, tb), tb)
+                pacc[zb, :, where] = jnp.zeros((hd, tb), F32)
+                tt[y, pl.ds(zb, 1), where] = jnp.zeros((1, tb), F32)
 
         @pl.when(jnp.logical_and(i > 0, i < nz - 1))
         def _():
@@ -340,20 +341,16 @@
         def _():
             relay_up(i - 2)
 
-    def down_step(step):
-        for h in range(2):
-            for i, to in ((2 * step - 1, right), (2 * step, left)):
-                zz = zof(i)
-                dmail.arrived(2 * i + h, down_half(zz, h), to)
-                if i + 2 < nz - 1:
-                    dmail.start(2 * (i + 2) + h, down_half(zz, h), down_half(zz, h), to)
-                elif (i + h) % 2 == 1:
-                    dmail.start(2 * (nz - 1) + h, down_half(zz, h), down_half(zz, h), to)
-
-    @pl.loop(0, rows // 128)
-    def _(n):
-        at = pl.ds(pl.multiple_of(n * 128, 128), 128)
-        tt[y, :, at] = tcol[at, :].T[:8, :]
+    def down_tick(step, h):
+        for i, to in ((2 * step - 1, right), (2 * step, left)):
+            zz = zof(i)
+            dmail.arrived(2 * i + h, down_half(zz, h), to)
+            if i + 2 < nz - 1:
+                dmail.start(2 * (i + 2) + h, down_half(zz, h), down_half(zz, h), to)
+            elif (i + h) % 2 == 1:
+                dmail.start(2 * (nz - 1) + h, down_half(zz, h), down_half(zz, h), to)
+
+    final = nz // 2 - 1
 
     for r in range(1, ny):
         mail.start(m_t + r, tt.at[y], tt.at[y], ydev(r))
@@ -376,49 +373,42 @@
         fac[zz : zz + 1, :] = jnp.exp2(-(beyond + after[zz : zz + 1, :]))
         beyond = beyond + every[zz : zz + 1, :]
 
-    chunk = min(128, half)
-    per = half // chunk
+    if final > 1:
+        down_tick(1, 0)
+    per = tb // 128
 
     @pl.loop(0, rows // 128)
     def _(n):
         at = pl.ds(pl.multiple_of(n * 128, 128), 128)
-        cols = fac[:, at].T
-        acc = cols[:, 0:1] * pacc[0, at, :]
+        acc = fac[0:1, at] * pacc[0, :, at]
         for zz in range(1, nz):
-            acc = acc + cols[:, zz : zz + 1] * pacc[zz, at, :]
-        partf[at, :] = acc
-        part[at, :] = acc.astype(BF16)
-
-    for r in range(1, ny):
-        for h in range(2):
-            to = lax.rem(y + r, ny)
-            src = part.at[pl.ds(pl.multiple_of((h * ny + to) * half, half), half), :]
-            mail.start(m_p + r if h == 0 else m_p2(m_p, r, g0, gn), src, prec.at[y, h], ydev(r))
+            acc = acc + fac[zz : zz + 1, at] * pacc[zz, :, at]
+        col = pl.ds(pl.multiple_of(lax.rem(n, per) * 128, 128), 128)
+        partf[n // per, :, col] = acc
+        part[n // per, :, col] = acc.astype(BF16)
+
+    for r in range(1, ny):
+        mail.start(m_p + r, part.at[lax.rem(y + r, ny)], prec.at[y], ydev(r))
     relay_up(nz - 2)
-    own = lambda h: partf[pl.ds(pl.multiple_of((h * ny + y) * half, half), half), :]
-
-    def summed(h):
-        acc = own(h)
+    for r in range(1, ny):
+        mail.arrived(m_p + r, prec.at[lax.rem(y + ny - r, ny)], ydev(r))
+    mycol = pl.ds(pl.multiple_of(me * hd, hd), hd)
+    for h in range(2):
+        side = slice(h * half, (h + 1) * half)
+        acc = partf[y, :, side]
         for r in range(1, ny):
-            frm = lax.rem(y + ny - r, ny)
-            mail.arrived(m_p + r if h == 0 else m_p2(m_p, r, g0, gn), prec.at[frm, h], ydev(r))
-            acc = acc + prec[frm, h].astype(F32)
-        return acc.astype(BF16)
-
-    mycol = pl.ds(pl.multiple_of(me * hd, hd), hd)
-    stage[...] = summed(1)
-    mail.start(m_ret, stage, att_full.at[pl.ds(half, half), mycol], mirror)
+            acc = acc + prec[lax.rem(y + r, ny), :, side].astype(F32)
+        att_full[side, mycol] = acc.T.astype(BF16)
+        g_att[h].start(att_full.at[pl.ds(h * half, half), mycol])
     relay_up(nz - 1)
-    att_full[:half, mycol] = summed(0)
-    g_att[0].start(att_full.at[pl.ds(0, half), mycol])
-    if nz > 4:
-        down_step(1)
-    mail.arrived(m_ret, att_full.at[pl.ds(half, half), mycol], mirror)
-    g_att[1].start(att_full.at[pl.ds(half, half), mycol])
+    if final > 1:
+        down_tick(1, 1)
     g_ow.finish()
     g_res.finish()
     g_att[0].forward()
     g_att[1].forward()
+    if final > 2:
+        down_tick(2, 0)
     g_att[0].finish()
     g_att[1].finish()
 
@@ -432,8 +422,8 @@
             ALPHA * res_full[:, at].astype(F32)
         )
 
-    if nz > 6:
-        down_step(2)
+    if final > 2:
+        down_tick(2, 1)
     rc = 64
 
     @pl.loop(0, tb // rc)
@@ -501,13 +491,13 @@
             def _():
                 mine[...] = both
 
-    final = nz // 2 - 1
+    down_tick(final, 0)
 
     @pl.loop(0, nz)
     def _(i):
         @pl.when(i == nz - 3)
         def _():
-            down_step(final)
+            down_tick(final, 1)
 
         @pl.when(i == nz - 1)
         def _():
@@ -550,29 +540,25 @@
             + shift2_ref[:, at]
         ).astype(BF16)
 
-    mail.sent(m_q2, late, mirror)
-    for r in range(1, ny):
-        mail.sent(m_q1 + r, early, mirror)
-        mail.sent(m_q2f + r, early, mirror)
-        mail.sent(m_t + r, tt.at[y], mirror)
-        mail.sent(m_p + r, stage, mirror)
-        mail.sent(m_p2(m_p, r, g0, gn), stage, mirror)
+    for r in range(1, ny):
+        mail.sent(m_q + r, q_ref, left)
+        mail.sent(m_t + r, tt.at[y], left)
+        mail.sent(m_p + r, prec.at[y], left)
     for r in range(1, nz):
-        mail.sent(m_b + r, b_ref, mirror)
-    mail.sent(m_ret, stage, mirror)
-    for r in range(1, ny):
-        mail.sent(m_d + r, dw_ref, mirror)
+        mail.sent(m_b + r, bb.at[z], left)
+    for r in range(1, ny):
+        mail.sent(m_d + r, dw_ref, left)
     for i in range(1, nz + 1):
-        umail.sent(i, up_slab(0, 0) if i < nz - 1 else up_slab(0, 0, 0), mirror)
+        umail.sent(i, up_slab(0, 0) if i < nz - 1 else up_slab(0, 0, 0), left)
     for i in range(nz):
-        ymail.sent(4 * i, up_slab(0, 0), mirror)
+        ymail.sent(4 * i, up_slab(0, 0), left)
         if ny > 2:
-            ymail.sent(4 * i + 1, up_slab(0, 0), mirror)
-            ymail.sent(4 * i + 2, up_slab(0, 0, 0), mirror)
-            ymail.sent(4 * i + 3, up_slab(0, 0, 0), mirror)
+            ymail.sent(4 * i + 1, up_slab(0, 0), left)
+            ymail.sent(4 * i + 2, up_slab(0, 0, 0), left)
+            ymail.sent(4 * i + 3, up_slab(0, 0, 0), left)
     for i in range(1, nz):
         for h in range(2):
-            dmail.sent(2 * i + h, down_half(0, 0), mirror)
+            dmail.sent(2 * i + h, down_half(0, 0), left)
     for n in range(nx):
         smail.sent(n, sbuf.at[0], sibling)
     for r in range(1, nx):
@@ -582,26 +568,22 @@
 
     @pl.loop(1, nz)
     def _(i):
-        kmail.sent(i, kb.at[0], mirror)
-        vmail.sent(i, vb.at[0], mirror)
+        kmail.sent(i, kb.at[0], left)
+        vmail.sent(i, vb.at[0], left)
 
     for g in [g_ow, g_res] + g_att:
         g.drain()
-
-
-def m_p2(m_p, r, g0, gn):
-    return g0 + 4 * gn + r
 
 
 def layer(nz, ny, nx, q, k, v, bias, ow, res, gain, shift, uw, dw, gain2, shift2):
     tb, hd = q.shape
     half = tb // 2
-    rows = 2 * ny * half
+    rows = ny * tb
     width = ow.shape[1]
     ntp = 2 * nx
     fw = width // ntp
     hidden = uw.shape[1]
-    messages = 3 * ny + nz + 2 * ny + 1 + ny + 4 * Gather.count(nx) + ny
+    messages = 4 * ny + nz + 4 * Gather.count(nx)
     vm = pl.BlockSpec(memory_space=pltpu.VMEM)
     dma = pltpu.SemaphoreType.DMA
     pairs = [messages, nz, nz, nz + 1, 4 * nz, 2 * nz, nx, nx, ntp]
@@ -611,19 +593,17 @@
         in_specs=[vm] * 12,
         out_specs=vm,
         scratch_shapes=[
-            pltpu.VMEM((2 * ny, half, hd), BF16),
+            pltpu.VMEM((ny, tb, hd), BF16),
             pltpu.VMEM((nz, tb, hd), BF16),
-            pltpu.VMEM((nz, tb, hd), BF16),
+            pltpu.VMEM((nz, hd, tb), BF16),
             pltpu.VMEM((nz, 8, tb), F32),
             pltpu.VMEM((tb, tb), BF16),
-            pltpu.VMEM((nz, rows, hd), F32),
-            pltpu.VMEM((rows, 128), F32),
-            pltpu.VMEM((ny, 8, rows), F32),
-            pltpu.VMEM((128, rows), F32),
-            pltpu.VMEM((rows, hd), BF16),
-            pltpu.VMEM((rows, hd), F32),
-            pltpu.VMEM((ny, 2, half, hd), BF16),
-            pltpu.VMEM((half, hd), BF16),
+            pltpu.VMEM((nz, hd, rows), F32),
+            pltpu.VMEM((ny, nz, rows), F32),
+            pltpu.VMEM((nz, rows), F32),
+            pltpu.VMEM((ny, hd, tb), BF16),
+            pltpu.VMEM((ny, hd, tb), F32),
+            pltpu.VMEM((ny, hd, tb), BF16),
             pltpu.VMEM((ntp * hd, width), BF16),
             pltpu.VMEM((tb, width), BF16),
             pltpu.VMEM((tb, ntp * hd), BF16),
@@ -651,10 +631,9 @@
 
 def body(nz, ny, nx, queries, keys, values, breaks, residual_in, out_weight, first_gain,
          first_shift, up_weight, down_weight, second_gain, second_shift):
-    bias = jnp.broadcast_to((breaks.astype(F32) * LOG2E).reshape(1, -1), (8, breaks.shape[0]))
     row = lambda a: a.reshape(1, -1)
     return layer(
-        nz, ny, nx, queries, keys, values, bias, out_weight, residual_in,
+        nz, ny, nx, queries, keys, values, row(breaks), out_weight, residual_in,
         row(first_gain), row(first_shift), up_weight, down_weight, row(second_gain), row(second_shift),
     )
 

time: 138 us -> 119 us (0.86)
  Pallas kernels: 135 us -> 117 us
    pallas_call x1, Pallas kernels: 135 us -> 117 us  [layer(): pl.pallas_call(functools.partial(layer_kernel, nz, ny, nx), out_shape=jax...]
where the time goes in v3:
time: 119 us
  Pallas kernels  117 us (98%)
  local copies, waits for them, and re-layouts  1.67 us (1%)
    pallas_call x1, Pallas kernels, layer(): pl.pallas_call(functools.partial(layer_kernel, nz, ny, nx), out_shape=jax...  117 us

profile of v3, /device:TPU:1, one launch (start us, length us, event | category | flops | bytes accessed | tf_op | source)
XLA Modules:
  0.0 118.9 jit_solution(3885751117193986370)
XLA Ops:
  0.0 117.3 %layer.1 = bf16[512,256]{1,0:T(8,128)(2,1)} custom-call(bf16[512,128]{1,0:T(8,128)(2,1)} %q_ref.1, bf16[512,128]{1,0:T(8,128)(2,1)} %k_ref.1, bf16[512,128]{1,0:T(8,128)(2,1)} %v_ref.1, bf16[1,512]{1,0:T(2,128)(2,1)} %bitcast.9, bf16[128,2048]{1,0:T(8,128)(2,1)} %ow_ref.1, bf16[512,256]{1,0:T(8,128)(2,1)} %res_ref.1, f32[1,2048]{1,0:T(1,128)} %bitcast.5, ...), custom_call_target="tpu_custom_call" | custom-call | tf_op jit(solution)/shard_map/layer/pallas_call | solution.py:590
  117.3 1.7 %copy.14 = bf16[512,256]{1,0:T(8,128)(2,1)} copy(bf16[512,256]{1,0:T(8,128)(2,1)} %layer.1) | data formatting | bytes 524288

commit v4 on v3

--- a/solution.py
+++ b/solution.py
@@ -96,7 +96,7 @@
     out_ref,
     qbuf, kb, vb, bb, tri, pacc, tt, fac, part, partf, prec,
     ow_full, res_full, att_full, pre, fo_ref,
-    up_full, down_full, act, hold, sbuf, sib, xbuf, rbuf, mine, cols, stat,
+    up_full, down_full, act, sbuf, sib, xbuf, rbuf, mine, cols, stat,
     msend, mrecv, ksend, krecv, vsend, vrecv,
     usend, urecv, ysend, yrecv, dsend, drecv,
     ssend, srecv, xsend, xrecv, tsend, trecv,
@@ -111,6 +111,7 @@
     kmail, vmail = Mail(ksend, krecv), Mail(vsend, vrecv)
     umail, ymail, dmail = Mail(usend, urecv), Mail(ysend, yrecv), Mail(dsend, drecv)
     wr = uw_ref.shape[0]
+    dw = res_ref.shape[1]
 
     def zdev(zz):
         return {"sp": zz * ny + y}
@@ -145,17 +146,25 @@
         pl.semaphore_signal(
             barrier, inc=1, device_id={"tp": lax.rem(me + r, 2 * nx)}, device_id_type=MESH
         )
+    vb[0] = v_ref[...].T
+    bb[z] = jnp.broadcast_to(b_ref[...].astype(F32) * LOG2E, (8, tb))
+    qbuf[y] = q_ref[...]
+    kb[0] = k_ref[...]
+    up_slab(z, 0)[...] = uw_ref[...]
+    down_slab(0)[...] = dw_ref[...]
+    ow_full[pl.ds(me * hd, hd), :] = ow_ref[...]
+    res_full[:, pl.ds(pl.multiple_of(me * dw, dw), dw)] = res_ref[...]
+    tri[...] = (iota((tb, tb), 0) > iota((tb, tb), 1)).astype(BF16)
     pl.semaphore_wait(barrier, nz - 1 + ny - 1 + 2 * nx - 1)
 
     m_q = 0
     m_b = ny
     m_t = m_b + nz
     m_p = m_t + ny
-    m_d = m_p + ny
+    m_d = m_p + 2 * ny
     g0 = m_d + ny
     gn = Gather.count(nx)
     g_ow = Gather(mail, g0, lambda j: ow_full.at[pl.ds(j * hd, hd), :], nx)
-    dw = res_ref.shape[1]
     g_res = Gather(
         mail, g0 + gn, lambda j: res_full.at[:, pl.ds(pl.multiple_of(j * dw, dw), dw)], nx
     )
@@ -176,8 +185,6 @@
     kmail.start(2, k_ref, kb.at[2], left)
     for r in range(1, ny):
         mail.start(m_q + r, q_ref, qbuf.at[y], ydev(r))
-    vb[0] = v_ref[...].T
-    bb[z] = jnp.broadcast_to(b_ref[...].astype(F32) * LOG2E, (8, tb))
     vmail.start(1, vb.at[0], vb.at[1], right)
     vmail.start(2, vb.at[0], vb.at[2], left)
     for r in range(1, nz):
@@ -212,15 +219,51 @@
     pass_up(0, uw_ref)
     g_ow.start(ow_ref)
     g_res.start(res_ref)
-    up_slab(z, 0)[...] = uw_ref[...]
-    down_slab(0)[...] = dw_ref[...]
-
-    qbuf[y] = q_ref[...]
-    kb[0] = k_ref[...]
-    ow_full[pl.ds(me * hd, hd), :] = ow_ref[...]
-    res_full[:, pl.ds(pl.multiple_of(me * dw, dw), dw)] = res_ref[...]
-    tri[...] = (iota((tb, tb), 0) > iota((tb, tb), 1)).astype(BF16)
-
+
+    def onward(i):
+        return zdev(lax.rem(jnp.where(lax.rem(i, 2) == 1, z + 1, z - 1) + nz, nz))
+
+    def pass_keys(i):
+        to = onward(i)
+        kmail.arrived(i, kb.at[i], to)
+
+        @pl.when(i <= nz - 4)
+        def _():
+            kmail.start(i + 2, kb.at[i], kb.at[i + 2], to)
+
+        @pl.when(i == nz - 3)
+        def _():
+            kmail.start(nz - 1, kb.at[i], kb.at[nz - 1], to)
+
+        vmail.arrived(i, vb.at[i], to)
+
+        @pl.when(i <= nz - 4)
+        def _():
+            vmail.start(i + 2, vb.at[i], vb.at[i + 2], to)
+
+        @pl.when(i == nz - 2)
+        def _():
+            vmail.start(nz - 1, vb.at[i], vb.at[nz - 1], to)
+
+    def ring_up(i):
+        to = onward(i)
+        zz = zof(i)
+        umail.arrived(i, up_slab(zz, 0), to)
+
+        @pl.when(i <= nz - 4)
+        def _():
+            umail.start(i + 2, up_slab(zz, 0), up_slab(zz, 0), to)
+
+        @pl.when(i == nz - 3)
+        def _():
+            umail.start(nz - 1, up_slab(zz, 0, 0), up_slab(zz, 0, 0), to)
+
+        @pl.when(i == nz - 2)
+        def _():
+            umail.start(nz, up_slab(zz, 0, 1), up_slab(zz, 0, 1), to)
+
+    for i in (1, 2):
+        pass_keys(jnp.int32(i))
     for r in range(1, ny):
         mail.arrived(m_q + r, qbuf.at[lax.rem(y + ny - r, ny)], ydev(r))
     for r in range(1, nz):
@@ -234,25 +277,13 @@
     def _(i):
         odd = lax.rem(i, 2)
         zb = zof(i)
-        onward = zdev(lax.rem(jnp.where(odd == 1, z + 1, z - 1) + nz, nz))
-
-        @pl.when(i > 0)
-        def _():
-            kmail.arrived(i, kb.at[i], onward)
-            vmail.arrived(i, vb.at[i], onward)
-
-        @pl.when(jnp.logical_and(i >= 1, i <= nz - 4))
-        def _():
-            kmail.start(i + 2, kb.at[i], kb.at[i + 2], onward)
-            vmail.start(i + 2, vb.at[i], vb.at[i + 2], onward)
-
-        @pl.when(i == nz - 3)
-        def _():
-            kmail.start(nz - 1, kb.at[i], kb.at[nz - 1], onward)
-
-        @pl.when(i == nz - 2)
-        def _():
-            vmail.start(nz - 1, vb.at[i], vb.at[nz - 1], onward)
+        @pl.when(jnp.logical_and(odd == 1, i > 1))
+        def _():
+            pass_keys(i)
+
+            @pl.when(i + 1 < nz)
+            def _():
+                pass_keys(i + 1)
 
         def tile(t, masked):
             def scored(h):
@@ -288,54 +319,63 @@
                 total = lax.dot_general(ones, soft16, NT, preferred_element_type=F32)
                 tt[y, pl.ds(zb, 1), where] = total[0:1, :]
 
-            both = [scored(h) for h in range(2)]
-            weights = [weighed(h, *both[h]) for h in range(2)]
-            for h in range(2):
-                finish(h, both[h][1], *weights[h])
-
-        @pl.loop(0, ny)
-        def _(t):
-            qblock = z * ny + t
-            kblock = zb * ny + y
-
-            @pl.when(kblock < qblock)
-            def _():
-                tile(t, False)
-
-            @pl.when(kblock == qblock)
-            def _():
-                tile(t, True)
-
-            @pl.when(kblock > qblock)
-            def _():
-                where = pl.ds(pl.multiple_of(t * tb, tb), tb)
-                pacc[zb, :, where] = jnp.zeros((hd, tb), F32)
-                tt[y, pl.ds(zb, 1), where] = jnp.zeros((1, tb), F32)
-
-        @pl.when(jnp.logical_and(i > 0, i < nz - 1))
-        def _():
-            umail.arrived(i, up_slab(zb, 0), onward)
-
-        @pl.when(jnp.logical_and(i >= 1, i <= nz - 4))
-        def _():
-            umail.start(i + 2, up_slab(zb, 0), up_slab(zb, 0), onward)
+            return scored, weighed, finish
+
+        def run(tiles):
+            stage1, stage2 = {}, {}
+            parts = [(fns, h) for fns in tiles for h in range(2)]
+            for n in range(len(parts) + 2):
+                if n < len(parts):
+                    fns, h = parts[n]
+                    stage1[n] = fns[0](h)
+                if 0 <= n - 1 < len(parts):
+                    fns, h = parts[n - 1]
+                    stage2[n - 1] = fns[1](h, *stage1[n - 1])
+                if 0 <= n - 2:
+                    fns, h = parts[n - 2]
+                    fns[2](h, stage1[n - 2][1], *stage2[n - 2])
+
+        @pl.when(zb < z)
+        def _():
+            run([tile(t, False) for t in range(ny)])
+
+        @pl.when(zb > z)
+        def _():
+            pacc[zb] = jnp.zeros((hd, rows), F32)
+            tt[y, pl.ds(zb, 1), :] = jnp.zeros((1, rows), F32)
+
+        @pl.when(zb == z)
+        def _():
+            @pl.loop(0, ny)
+            def _(t):
+                @pl.when(t > y)
+                def _():
+                    run([tile(t, False)])
+
+                @pl.when(t == y)
+                def _():
+                    run([tile(t, True)])
+
+                @pl.when(t < y)
+                def _():
+                    where = pl.ds(pl.multiple_of(t * tb, tb), tb)
+                    pacc[zb, :, where] = jnp.zeros((hd, tb), F32)
+                    tt[y, pl.ds(zb, 1), where] = jnp.zeros((1, tb), F32)
+
+        @pl.when(jnp.logical_and(odd == 1, i < nz - 1))
+        def _():
+            for n in (i, i + 1):
+                ring_up(n)
+            for n in (i, i + 1):
+                pass_up(n, None)
 
         @pl.when(i == nz - 3)
         def _():
-            umail.start(nz - 1, up_slab(zb, 0, 0), up_slab(zb, 0, 0), onward)
-
-        @pl.when(i == nz - 2)
-        def _():
-            umail.start(nz, up_slab(zb, 0, 1), up_slab(zb, 0, 1), onward)
             for r in range(1, ny):
                 mail.arrived(m_d + r, down_slab(-r), ydev(r))
             for h in range(2):
                 for j, to in ((1, right), (2, left)):
                     dmail.start(2 * j + h, down_half(z, h), down_half(z, h), to)
-
-        @pl.when(jnp.logical_and(i > 0, i < nz - 1))
-        def _():
-            pass_up(i, None)
 
         @pl.when(i >= 2)
         def _():
@@ -354,10 +394,6 @@
 
     for r in range(1, ny):
         mail.start(m_t + r, tt.at[y], tt.at[y], ydev(r))
-    last = zof(nz - 1)
-    umail.arrived(nz - 1, up_slab(last, 0, 0), left)
-    umail.arrived(nz, up_slab(last, 0, 1), right)
-    pass_up(nz - 1, None)
     g_ow.forward()
     g_res.forward()
     for r in range(1, ny):
@@ -375,145 +411,165 @@
 
     if final > 1:
         down_tick(1, 0)
-    per = tb // 128
-
-    @pl.loop(0, rows // 128)
-    def _(n):
-        at = pl.ds(pl.multiple_of(n * 128, 128), 128)
-        acc = fac[0:1, at] * pacc[0, :, at]
-        for zz in range(1, nz):
-            acc = acc + fac[zz : zz + 1, at] * pacc[zz, :, at]
-        col = pl.ds(pl.multiple_of(lax.rem(n, per) * 128, 128), 128)
-        partf[n // per, :, col] = acc
-        part[n // per, :, col] = acc.astype(BF16)
-
-    for r in range(1, ny):
-        mail.start(m_p + r, part.at[lax.rem(y + r, ny)], prec.at[y], ydev(r))
-    relay_up(nz - 2)
-    for r in range(1, ny):
-        mail.arrived(m_p + r, prec.at[lax.rem(y + ny - r, ny)], ydev(r))
+    per = half // 128 if half >= 128 else 1
+    wc = min(128, half)
+
+    for h in range(2):
+
+        @pl.loop(0, ny * per)
+        def _(n):
+            to = n // per
+            off = lax.rem(n, per) * wc
+            at = pl.ds(pl.multiple_of(to * tb + h * half + off, wc), wc)
+            acc = fac[0:1, at] * pacc[0, :, at]
+            for zz in range(1, nz):
+                acc = acc + fac[zz : zz + 1, at] * pacc[zz, :, at]
+            col = pl.ds(pl.multiple_of(off, wc), wc)
+            partf[h, to, :, col] = acc
+            part[h, to, :, col] = acc.astype(BF16)
+
+        for r in range(1, ny):
+            mail.start(m_p + h * ny + r, part.at[h, lax.rem(y + r, ny)], prec.at[h, y], ydev(r))
+
+    last = zof(nz - 1)
+    umail.arrived(nz - 1, up_slab(last, 0, 0), left)
+    umail.arrived(nz, up_slab(last, 0, 1), right)
+    pass_up(nz - 1, None)
     mycol = pl.ds(pl.multiple_of(me * hd, hd), hd)
     for h in range(2):
-        side = slice(h * half, (h + 1) * half)
-        acc = partf[y, :, side]
+        acc = partf[h, y]
         for r in range(1, ny):
-            acc = acc + prec[lax.rem(y + r, ny), :, side].astype(F32)
-        att_full[side, mycol] = acc.T.astype(BF16)
+            frm = lax.rem(y + ny - r, ny)
+            mail.arrived(m_p + h * ny + r, prec.at[h, frm], ydev(r))
+            acc = acc + prec[h, frm].astype(F32)
+        att_full[h * half : (h + 1) * half, mycol] = acc.T.astype(BF16)
         g_att[h].start(att_full.at[pl.ds(h * half, half), mycol])
-    relay_up(nz - 1)
+    relay_up(nz - 2)
+    g_ow.finish()
+    g_res.finish()
     if final > 1:
         down_tick(1, 1)
-    g_ow.finish()
-    g_res.finish()
     g_att[0].forward()
     g_att[1].forward()
-    if final > 2:
-        down_tick(2, 0)
-    g_att[0].finish()
-    g_att[1].finish()
+    relay_up(nz - 1)
 
     width = ow_full.shape[1]
     nc = min(256, width)
-
-    @pl.loop(0, width // nc)
-    def _(n):
-        at = pl.ds(pl.multiple_of(n * nc, nc), nc)
-        pre[:, at] = jnp.dot(att_full[...], ow_full[:, at], preferred_element_type=F32) + (
-            ALPHA * res_full[:, at].astype(F32)
-        )
-
-    if final > 2:
-        down_tick(2, 1)
     rc = 64
-
-    @pl.loop(0, tb // rc)
-    def _(n):
-        at = pl.ds(pl.multiple_of(n * rc, rc), rc)
-        row = pre[at, :]
-        center = jnp.mean(row, axis=-1, keepdims=True)
-        off = row - center
-        spread = jnp.mean(off * off, axis=-1, keepdims=True)
-        fo_ref[at, :] = (off * lax.rsqrt(spread + EPSILON) * gain_ref[...] + shift_ref[...]).astype(
-            BF16
-        )
-
-    for i in range(nz):
-        take_up(i)
     hidden = up_full.shape[1]
     hc = min(256, hidden)
-
-    @pl.loop(0, hidden // hc)
-    def _(n):
-        at = pl.ds(pl.multiple_of(n * hc, hc), hc)
-        h = jnp.maximum(jnp.dot(fo_ref[...], up_full[:, at], preferred_element_type=F32), 0.0)
-        act[:, at] = (h * h).astype(BF16)
-
     ntp = 2 * nx
     x, c = me // 2, lax.rem(me, 2)
     smail, xmail, tmail = Mail(ssend, srecv), Mail(xsend, xrecv), Mail(tsend, trecv)
     sibling = {"tp": x * 2 + 1 - c}
     fw = out_ref.shape[1]
 
-    def mix(i):
-        j = zof(i)
-        chip = j // 2
-        piece = lax.dot_general(
-            act[...],
+    def project(h):
+        side = slice(h * half, (h + 1) * half)
+
+        @pl.loop(0, width // nc)
+        def _(n):
+            at = pl.ds(pl.multiple_of(n * nc, nc), nc)
+            pre[side, at] = jnp.dot(
+                att_full[side, :], ow_full[:, at], preferred_element_type=F32
+            ) + ALPHA * res_full[side, at].astype(F32)
+
+        @pl.loop(0, half // rc)
+        def _(n):
+            at = pl.ds(pl.multiple_of(h * half + n * rc, rc), rc)
+            row = pre[at, :]
+            center = jnp.mean(row, axis=-1, keepdims=True)
+            off = row - center
+            spread = jnp.mean(off * off, axis=-1, keepdims=True)
+            fo_ref[at, :] = (
+                off * lax.rsqrt(spread + EPSILON) * gain_ref[...] + shift_ref[...]
+            ).astype(BF16)
+
+    def lift(h):
+        side = slice(h * half, (h + 1) * half)
+
+        @pl.loop(0, hidden // hc)
+        def _(n):
+            at = pl.ds(pl.multiple_of(n * hc, hc), hc)
+            up = jnp.maximum(
+                jnp.dot(fo_ref[side, :], up_full[:, at], preferred_element_type=F32), 0.0
+            )
+            act[side, at] = (up * up).astype(BF16)
+
+    def piece(j, h):
+        return lax.dot_general(
+            act[h * half : (h + 1) * half, :],
             down_full[pl.ds(pl.multiple_of(j * fw, fw), fw), :],
             NT,
             preferred_element_type=F32,
         )
 
-        @pl.when(lax.rem(j, 2) != c)
-        def _():
-            sbuf[chip] = piece.astype(BF16)
-            smail.start(chip, sbuf.at[chip], sib.at[chip], sibling)
-
-        @pl.when(lax.rem(j, 2) == c)
-        def _():
-            hold[...] = piece
-
-    def settle(i):
-        j = zof(i)
-        chip = j // 2
-
-        @pl.when(lax.rem(j, 2) == c)
-        def _():
-            smail.arrived(chip, sib.at[chip], sibling)
-            both = hold[...] + sib[chip].astype(F32)
-
-            @pl.when(chip != x)
+    def mix(lo, hi, halves):
+        @pl.loop(lo, hi)
+        def _(i):
+            j = zof(i)
+            chip = j // 2
+
+            @pl.when(lax.rem(j, 2) != c)
             def _():
-                xbuf[chip] = both.astype(BF16)
-                xmail.start(chip, xbuf.at[chip], rbuf.at[x], {"tp": j}, there=x)
-
-            @pl.when(chip == x)
+                for h in halves:
+                    sbuf[h, chip] = piece(j, h).astype(BF16)
+                    m = 2 * chip + h
+                    smail.start(m, sbuf.at[h, chip], sib.at[h, chip], sibling)
+
+        @pl.loop(lo, hi)
+        def _(i):
+            j = zof(i)
+            chip = j // 2
+
+            @pl.when(lax.rem(j, 2) == c)
             def _():
-                mine[...] = both
-
+                for h in halves:
+                    own = piece(j, h)
+                    m = 2 * chip + h
+                    smail.arrived(m, sib.at[h, chip], sibling)
+                    both = own + sib[h, chip].astype(F32)
+
+                    @pl.when(chip != x)
+                    def _():
+                        xbuf[h, chip] = both.astype(BF16)
+                        xmail.start(
+                            m, xbuf.at[h, chip], rbuf.at[h, x], {"tp": j}, there=2 * x + h
+                        )
+
+                    @pl.when(chip == x)
+                    def _():
+                        mine[h * half : (h + 1) * half, :] = both
+
+    early = nz - 3
+    for h in range(2):
+        g_att[h].finish()
+        project(h)
+        if h == 0:
+            for i in range(nz):
+                take_up(i)
+            if final > 2:
+                down_tick(2, 0)
+        lift(h)
+        if final > 2 and h == 0:
+            down_tick(2, 1)
+        mix(0, early, (h,))
     down_tick(final, 0)
-
-    @pl.loop(0, nz)
-    def _(i):
-        @pl.when(i == nz - 3)
-        def _():
-            down_tick(final, 1)
-
-        @pl.when(i == nz - 1)
-        def _():
-            zz = zof(nz - 1)
-            dmail.arrived(2 * (nz - 1), down_half(zz, 0), left)
-            dmail.arrived(2 * (nz - 1) + 1, down_half(zz, 1), right)
-
-        mix(i)
-        settle(i)
+    down_tick(final, 1)
+    mix(early, nz - 1, (0, 1))
+    zz = zof(nz - 1)
+    dmail.arrived(2 * (nz - 1), down_half(zz, 0), left)
+    dmail.arrived(2 * (nz - 1) + 1, down_half(zz, 1), right)
+    mix(nz - 1, nz, (0, 1))
 
     at = pl.ds(pl.multiple_of(me * fw, fw), fw)
     mine[...] = mine[...] + ALPHA * fo_ref[:, at].astype(F32)
-    for r in range(1, nx):
-        n = lax.rem(x + r, nx)
-        xmail.arrived(n, rbuf.at[n], sibling)
-        mine[...] = mine[...] + rbuf[n].astype(F32)
+    for h in range(2):
+        side = slice(h * half, (h + 1) * half)
+        for r in range(1, nx):
+            n = lax.rem(x + r, nx)
+            xmail.arrived(2 * n + h, rbuf.at[h, n], sibling)
+            mine[side, :] = mine[side, :] + rbuf[h, n].astype(F32)
     total = mine[...]
     row_sum = jnp.sum(total, axis=-1, keepdims=True)
     row_squares = jnp.sum(total * total, axis=-1, keepdims=True)
@@ -543,7 +599,8 @@
     for r in range(1, ny):
         mail.sent(m_q + r, q_ref, left)
         mail.sent(m_t + r, tt.at[y], left)
-        mail.sent(m_p + r, prec.at[y], left)
+        mail.sent(m_p + r, prec.at[0, y], left)
+        mail.sent(m_p + ny + r, prec.at[0, y], left)
     for r in range(1, nz):
         mail.sent(m_b + r, bb.at[z], left)
     for r in range(1, ny):
@@ -559,10 +616,11 @@
     for i in range(1, nz):
         for h in range(2):
             dmail.sent(2 * i + h, down_half(0, 0), left)
-    for n in range(nx):
-        smail.sent(n, sbuf.at[0], sibling)
+    for n in range(2 * nx):
+        smail.sent(n, sbuf.at[0, 0], sibling)
     for r in range(1, nx):
-        xmail.sent(lax.rem(x + r, nx), rbuf.at[0], sibling)
+        for h in range(2):
+            xmail.sent(2 * lax.rem(x + r, nx) + h, rbuf.at[0, 0], sibling)
     for r in range(1, ntp):
         tmail.sent(r, stat.at[me], sibling)
 
@@ -583,10 +641,10 @@
     ntp = 2 * nx
     fw = width // ntp
     hidden = uw.shape[1]
-    messages = 4 * ny + nz + 4 * Gather.count(nx)
+    messages = 5 * ny + nz + 4 * Gather.count(nx)
     vm = pl.BlockSpec(memory_space=pltpu.VMEM)
     dma = pltpu.SemaphoreType.DMA
-    pairs = [messages, nz, nz, nz + 1, 4 * nz, 2 * nz, nx, nx, ntp]
+    pairs = [messages, nz, nz, nz + 1, 4 * nz, 2 * nz, 2 * nx, 2 * nx, ntp]
     return pl.pallas_call(
         functools.partial(layer_kernel, nz, ny, nx),
         out_shape=jax.ShapeDtypeStruct((tb, fw), BF16),
@@ -601,9 +659,9 @@
             pltpu.VMEM((nz, hd, rows), F32),
             pltpu.VMEM((ny, nz, rows), F32),
             pltpu.VMEM((nz, rows), F32),
-            pltpu.VMEM((ny, hd, tb), BF16),
-            pltpu.VMEM((ny, hd, tb), F32),
-            pltpu.VMEM((ny, hd, tb), BF16),
+            pltpu.VMEM((2, ny, hd, half), BF16),
+            pltpu.VMEM((2, ny, hd, half), F32),
+            pltpu.VMEM((2, ny, hd, half), BF16),
             pltpu.VMEM((ntp * hd, width), BF16),
             pltpu.VMEM((tb, width), BF16),
             pltpu.VMEM((tb, ntp * hd), BF16),
@@ -612,11 +670,10 @@
             pltpu.VMEM((width, hidden), BF16),
             pltpu.VMEM((width, hidden), BF16),
             pltpu.VMEM((tb, hidden), BF16),
-            pltpu.VMEM((tb, fw), F32),
-            pltpu.VMEM((nx, tb, fw), BF16),
-            pltpu.VMEM((nx, tb, fw), BF16),
-            pltpu.VMEM((nx, tb, fw), BF16),
-            pltpu.VMEM((nx, tb, fw), BF16),
+            pltpu.VMEM((2, nx, half, fw), BF16),
+            pltpu.VMEM((2, nx, half, fw), BF16),
+            pltpu.VMEM((2, nx, half, fw), BF16),
+            pltpu.VMEM((2, nx, half, fw), BF16),
             pltpu.VMEM((tb, fw), F32),
             pltpu.VMEM((tb, 128), F32),
             pltpu.VMEM((ntp, 8, tb), F32),

time: 119 us -> 116 us (0.975)
  Pallas kernels: 117 us -> 114 us
    pallas_call x1, Pallas kernels: 117 us -> 114 us  [layer(): pl.pallas_call(functools.partial(layer_kernel, nz, ny, nx), out_shape=jax...]
where the time goes in v4:
time: 116 us; the launch traced here: 115 us
  Pallas kernels  114 us (98%)
  local copies, waits for them, and re-layouts  1.67 us (1%)
    pallas_call x1, Pallas kernels, layer(): pl.pallas_call(functools.partial(layer_kernel, nz, ny, nx), out_shape=jax...  114 us

profile of v4, /device:TPU:1, one launch (start us, length us, event | category | flops | bytes accessed | tf_op | source)
XLA Modules:
  0.0 115.4 jit_solution(407815638728533560)
XLA Ops:
  0.0 113.7 %layer.1 = bf16[512,256]{1,0:T(8,128)(2,1)} custom-call(bf16[512,128]{1,0:T(8,128)(2,1)} %q_ref.1, bf16[512,128]{1,0:T(8,128)(2,1)} %k_ref.1, bf16[512,128]{1,0:T(8,128)(2,1)} %v_ref.1, bf16[1,512]{1,0:T(2,128)(2,1)} %bitcast.9, bf16[128,2048]{1,0:T(8,128)(2,1)} %ow_ref.1, bf16[512,256]{1,0:T(8,128)(2,1)} %res_ref.1, f32[1,2048]{1,0:T(1,128)} %bitcast.5, ...), custom_call_target="tpu_custom_call" | custom-call | tf_op jit(solution)/shard_map/layer/pallas_call | solution.py:648
  113.7 1.7 %copy.14 = bf16[512,256]{1,0:T(8,128)(2,1)} copy(bf16[512,256]{1,0:T(8,128)(2,1)} %layer.1) | data formatting | bytes 524288

commit v5 on v4

--- a/solution.py
+++ b/solution.py
@@ -128,6 +128,9 @@
         n = wr if part is None else wr // 2
         return up_full.at[pl.ds(pl.multiple_of(at + (part or 0) * n, n), n), :]
 
+    def break_row(zz):
+        return bb.at[zz, pl.ds(0, 1)]
+
     dh = ny * wr // 2
 
     def down_half(zz, h):
@@ -188,7 +191,7 @@
     vmail.start(1, vb.at[0], vb.at[1], right)
     vmail.start(2, vb.at[0], vb.at[2], left)
     for r in range(1, nz):
-        mail.start(m_b + r, bb.at[z], bb.at[z], zdev(lax.rem(z + r, nz)))
+        mail.start(m_b + r, break_row(z), break_row(z), zdev(lax.rem(z + r, nz)))
     umail.start(1, uw_ref, up_slab(z, 0), right)
     umail.start(2, uw_ref, up_slab(z, 0), left)
     for r in range(1, ny):
@@ -267,7 +270,7 @@
     for r in range(1, ny):
         mail.arrived(m_q + r, qbuf.at[lax.rem(y + ny - r, ny)], ydev(r))
     for r in range(1, nz):
-        mail.arrived(m_b + r, bb.at[lax.rem(z + nz - r, nz)], left)
+        mail.arrived(m_b + r, break_row(lax.rem(z + nz - r, nz)), left)
 
     scale = hd ** (-0.5) * LOG2E
     hk = tb // 2
@@ -289,7 +292,7 @@
             def scored(h):
                 q = qbuf[t, h * half : (h + 1) * half, :]
                 scores = lax.dot_general(q, kb[i], NT, preferred_element_type=F32)
-                logits = scores * scale + bb[zb][0:1, :]
+                logits = scores * scale + bb[zb, 0:1, :]
                 soft = jnp.maximum(
                     jnp.log(1.0 + jnp.exp2(jnp.minimum(logits, CLAMP))) * LOG2E, logits
                 )
@@ -602,7 +605,7 @@
         mail.sent(m_p + r, prec.at[0, y], left)
         mail.sent(m_p + ny + r, prec.at[0, y], left)
     for r in range(1, nz):
-        mail.sent(m_b + r, bb.at[z], left)
+        mail.sent(m_b + r, break_row(z), left)
     for r in range(1, ny):
         mail.sent(m_d + r, dw_ref, left)
     for i in range(1, nz + 1):

time: 116 us -> 115 us (level)
  no operation moved by 1% of the time
where the time goes in v5:
time: 115 us
  Pallas kernels  113 us (98%)
  local copies, waits for them, and re-layouts  1.67 us (1%)
    pallas_call x1, Pallas kernels, layer(): pl.pallas_call(functools.partial(layer_kernel, nz, ny, nx), out_shape=jax...  113 us

profile of v5, /device:TPU:1, one launch (start us, length us, event | category | flops | bytes accessed | tf_op | source)
XLA Modules:
  0.0 114.9 jit_solution(3778240558336044967)
XLA Ops:
  0.0 113.2 %layer.1 = bf16[512,256]{1,0:T(8,128)(2,1)} custom-call(bf16[512,128]{1,0:T(8,128)(2,1)} %q_ref.1, bf16[512,128]{1,0:T(8,128)(2,1)} %k_ref.1, bf16[512,128]{1,0:T(8,128)(2,1)} %v_ref.1, bf16[1,512]{1,0:T(2,128)(2,1)} %bitcast.9, bf16[128,2048]{1,0:T(8,128)(2,1)} %ow_ref.1, bf16[512,256]{1,0:T(8,128)(2,1)} %res_ref.1, f32[1,2048]{1,0:T(1,128)} %bitcast.5, ...), custom_call_target="tpu_custom_call" | custom-call | tf_op jit(solution)/shard_map/layer/pallas_call | solution.py:651
  113.2 1.7 %copy.14 = bf16[512,256]{1,0:T(8,128)(2,1)} copy(bf16[512,256]{1,0:T(8,128)(2,1)} %layer.1) | data formatting | bytes 524288
